TPU v7x, 512 devices: a whole 4x4x16 slice. The times are simulated.
512 devices in a mesh: sp: 32 (over z, core), tp: 16 (over y, x).
Axes of the slice: x: 4, y: 4, z: 16, core: 2. Of those that a mesh axis runs over, the one named last changes fastest.
Arguments:
- stream: bfloat16 [2048, 4096], P('tp', 'sp')
- values_in: bfloat16 [1024, 4096], P('tp', 'sp'), may hold values from -6 to 6
- in_gate: bfloat16 [1024, 4096], P('tp', 'sp'), may hold values from -6 to 6
- out_gate: bfloat16 [1024, 4096], P('tp', 'sp'), may hold values from -6 to 6
- documents: int32 [4096], P('sp'), may hold values from 0 to 63, never falling along the last dimension, each value on 1 to 256 neighbouring positions
- conv_taps: float32 [3, 1024], P(None, 'tp'), may hold values from -3.5 to 3.5
- head_gain: float32 [1024], P('tp'), may hold values from 0.1 to 1.9
- mix_weight: bfloat16 [1024, 2048], P('tp'), may hold values from -0.25 to 0.25
- norm_gain: float32 [2048], P('tp'), may hold values from 0.1 to 1.9
- routes: int32 [4096, 4], P('sp'), may hold values from 0 to 31, all different within a row; in each aligned block of 128 rows (0 to 127, 128 to 255, ...) at most 24 rows name the same one
- route_weight: float32 [4096, 4], P('sp'), may hold values from 0.2 to 1
- expert_gate: bfloat16 [32, 2048, 2048], P('sp', None, 'tp'), may hold values from -0.125 to 0.125
- expert_up: bfloat16 [32, 2048, 2048], P('sp', None, 'tp'), may hold values from -0.125 to 0.125
- expert_down: bfloat16 [32, 2048, 2048], P('sp', None, 'tp'), may hold values from -0.125 to 0.125
- shared_gate: bfloat16 [2048, 2048], P(None, 'tp'), may hold values from -0.125 to 0.125
- shared_up: bfloat16 [2048, 2048], P(None, 'tp'), may hold values from -0.125 to 0.125
- shared_down: bfloat16 [2048, 2048], P('tp'), may hold values from -0.1875 to 0.1875
Outputs:
- layer_out: bfloat16 [2048, 4096], P('tp', 'sp')
Inputs may be any that keep to these rules, and one draw needn't show every extreme that they name: `routes`: each row names 4 different experts. In each aligned block of 128 rows no expert is named by more than 24 rows, a bound that some block reaches. `documents`: document numbers never fall along the positions; each document has 1 to 256 positions, and one has exactly that many.
All inputs are finite; a program needn't handle non-finite values.
Results may differ from a plain program's by a relative error of at most 0.015.
Values may be sent and summed in bfloat16 or wider, within the bound.
A program may use at most 64 MiB of HBM per device.

v0:
```python
import jax
import jax.numpy as jnp
from jax import lax
from jax.sharding import Mesh
from jax.sharding import PartitionSpec as P

D = 2048
HEAD = 64
TP = ("tp_0", "tp_1")


epsilon = 1e-06


def from_behind(x, axis, by):
    size = lax.axis_size(axis)
    pairs = [(i, i + by) for i in range(size) if 0 <= i + by < size]
    return lax.ppermute(x, axis, pairs)


def in_blocks(x, dim, size):
    before, after = (x.shape[:dim], x.shape[dim + 1 :])
    return jnp.moveaxis(x.reshape(*before, size, -1, *after), dim, 0)


def sum_at_owner(x, axis, dim):
    pieces = in_blocks(x, dim, lax.axis_size(axis))
    arrived = lax.all_to_all(pieces, axis, split_axis=0, concat_axis=0, tiled=True)
    return arrived.astype(jnp.float32).sum(axis=0)


def from_everyone(x, axis):
    size = lax.axis_size(axis)
    return lax.all_to_all(jnp.broadcast_to(x[None], (size, *x.shape)), axis, 0, 0, tiled=True)


def taken_together(x, axis):
    everything = from_everyone(x, axis)
    return jnp.sum(everything, axis=0)


def joined_along(pieces, dim):
    pieces = jnp.moveaxis(pieces, 0, dim)
    shape = pieces.shape
    return pieces.reshape(*shape[:dim], shape[dim] * shape[dim + 1], *shape[dim + 2 :])


def gather_directly(x, axis, dim):
    pieces = from_everyone(x, axis)
    return joined_along(pieces, dim)


def gather_axes(x, axes, dim):
    if not axes:
        return x
    nearer = lax.all_gather(x, axes[-1], axis=dim, tiled=True)
    return gather_axes(nearer, axes[:-1], dim)


def contract_rows(left, right):
    return lax.dot_general(
        left, right, (((0,), (0,)), ((), ())), preferred_element_type=jnp.float32
    )


def local(
    stream,
    values_in,
    in_gate,
    out_gate,
    documents,
    conv_taps,
    head_gain,
    mix_weight,
    norm_gain,
    routes,
    route_weight,
    expert_gate,
    expert_up,
    expert_down,
    shared_gate,
    shared_up,
    shared_down,
):
    positions = stream.shape[1]
    feat_rows = stream.shape[0]
    sp_count = lax.axis_size("sp")
    top_count = routes.shape[1]
    capacity = 3 * positions * top_count // (2 * sp_count)
    slot_total = sp_count * capacity
    tails = jnp.stack([values_in[:, -2:], in_gate[:, -2:]])
    before, before_docs = from_behind((tails, documents[-2:]), "sp", 1)
    joined = jnp.concatenate([before, jnp.stack([values_in, in_gate])], axis=2).astype(jnp.float32)
    product = joined[0] * joined[1]
    doc_ids = jnp.concatenate([before_docs, documents])
    convolved = jnp.zeros((values_in.shape[0], positions), jnp.float32)
    for offset in range(3):
        same_doc = (doc_ids[offset : offset + positions] == documents).astype(jnp.float32)
        convolved = (
            convolved
            + conv_taps[offset][:, None]
            * product[:, offset : offset + positions]
            * same_doc[None, :]
        )
    mixed = out_gate.astype(jnp.float32) * convolved
    heads = mixed.reshape(-1, HEAD, positions)
    heads = heads * lax.rsqrt(jnp.mean(heads * heads, axis=1, keepdims=True) + epsilon)
    normed_heads = (heads.reshape(mixed.shape) * head_gain[:, None]).astype(jnp.bfloat16)
    mixer = sum_at_owner(contract_rows(mix_weight, normed_heads).astype(jnp.bfloat16), TP, 0)
    hidden_state = stream.astype(jnp.float32) + mixer
    squares = taken_together(jnp.sum(hidden_state * hidden_state, axis=0), TP)
    normed = (hidden_state * lax.rsqrt(squares / D + epsilon)[None, :] * norm_gain[:, None]).astype(
        jnp.bfloat16
    )
    full_rows = gather_directly(normed, TP, 0)
    shared_mid = (
        jax.nn.silu(contract_rows(shared_gate, full_rows)) * contract_rows(shared_up, full_rows)
    ).astype(jnp.bfloat16)
    shared = sum_at_owner(contract_rows(shared_down, shared_mid).astype(jnp.bfloat16), TP, 0)
    flat_routes = routes.reshape(-1)
    onehot = (flat_routes[:, None] == jnp.arange(sp_count, dtype=jnp.int32)[None, :]).astype(
        jnp.int32
    )
    earlier = jnp.cumsum(onehot, axis=0) - onehot
    slot = jnp.sum(earlier * onehot, axis=1)
    column = flat_routes * capacity + slot
    chosen = (column[:, None] == jnp.arange(slot_total, dtype=jnp.int32)[None, :]).reshape(
        positions, top_count, slot_total
    )
    dispatch = jnp.any(chosen, axis=1).astype(jnp.bfloat16)
    combine = jnp.sum(chosen.astype(jnp.float32) * route_weight[:, :, None], axis=1)
    sent = jnp.dot(normed, dispatch, preferred_element_type=jnp.float32).astype(jnp.bfloat16)
    arrived = lax.all_to_all(
        sent.reshape(feat_rows, sp_count, capacity), "sp", split_axis=1, concat_axis=1, tiled=True
    )
    block_rows = gather_axes(arrived.reshape(feat_rows, slot_total), TP, 0)
    gate_rows = expert_gate[0]
    up_rows = expert_up[0]
    gate = contract_rows(gate_rows, block_rows)
    upward = contract_rows(up_rows, block_rows)
    expert_mid = (jax.nn.silu(gate) * upward).astype(jnp.bfloat16)
    weight_rows = expert_down[0]
    summed = contract_rows(weight_rows, lax.all_gather(expert_mid, TP, axis=0, tiled=True)).astype(
        jnp.bfloat16
    )
    returned = lax.all_to_all(
        summed.reshape(feat_rows, sp_count, capacity), "sp", split_axis=1, concat_axis=1, tiled=True
    )
    routed = lax.dot_general(
        returned.reshape(feat_rows, slot_total).astype(jnp.float32),
        combine,
        (((1,), (1,)), ((), ())),
        precision=lax.Precision.HIGHEST,
        preferred_element_type=jnp.float32,
    )
    return (hidden_state + shared + routed).astype(jnp.bfloat16)


def solution(mesh):
    split = Mesh(mesh.devices.reshape(mesh.shape["sp"], 4, 4), ("sp", "tp_0", "tp_1"))
    in_specs = (
        P(TP, "sp"),
        P(TP, "sp"),
        P(TP, "sp"),
        P(TP, "sp"),
        P("sp"),
        P(None, TP),
        P(TP),
        P(TP, None),
        P(TP),
        P("sp", None),
        P("sp", None),
        P("sp", None, TP),
        P("sp", None, TP),
        P("sp", None, TP),
        P(None, TP),
        P(None, TP),
        P(TP, None),
    )
    out_specs = P(TP, "sp")
    return jax.shard_map(local, mesh=split, in_specs=in_specs, out_specs=out_specs, check_vma=False)
```

profile of v0, /device:TPU:1, one launch (start us, length us, event | category | flops | bytes accessed | tf_op | source)
XLA Modules:
  0.0 260.6 jit_solution(9237096032666451016)
XLA Ops:
  6.5 0.8 slice.51
  7.3 4.9 %collective-permute-start.1 = (s32[2]{0:T(128)S(1)}, s32[2]{0:T(128)S(1)}, u32[]{:S(2)}, u32[]{:S(2)}) collective-permute-start(s32[2]{0:T(128)S(1)} %slice.51), channel_id=1, source_target_pairs={{0,16},{16,32},{32,48},{48,64},{64,80},{80,96},{96,112},{112,128},... | collective-permute-start | bytes 32 | tf_op jit(solution)/shard_map/ppermute | solution.py:18
  12.2 0.8 slice.46
  13.1 0.8 slice.47
  14.0 1.9 collective-permute-start
  16.0 0.8 slice_bitcast_fusion.2
  16.8 0.8 copy.92
  17.7 0.7 pad_add_fusion
  18.4 0.7 compare_convert_fusion.1
  19.3 0.8 maximum_convert_fusion
  20.1 0.8 multiply_reduce_fusion.1
  21.0 1.4 fusion.1
  22.4 0.9 copy.106
  23.3 6.7 %all-to-all-start = ((bf16[16,128,128]{1,2,0:T(8,128)(2,1)}), bf16[16,128,128]{1,2,0:T(8,128)(2,1)S(1)}, u32[]{:S(2)}, u32[]{:S(2)}) async-start(bf16[16,128,128]{1,2,0:T(8,128)(2,1)} %bitcast.90), calls=%async_computation | async-start | bytes 1048576 | tf_op jit(solution)/shard_map/all_to_all | solution.py:28
  30.1 1.2 reduce-window.6
  31.9 8.8 %all-to-all-done = bf16[16,128,128]{1,2,0:T(8,128)(2,1)S(1)} async-done(((bf16[16,128,128]{1,2,0:T(8,128)(2,1)}), bf16[16,128,128]{1,2,0:T(8,128)(2,1)S(1)}, u32[]{:S(2)}, u32[]{:S(2)}) %all-to-all-start) | async-done | bytes 524320 | tf_op jit(solution)/shard_map/all_to_all | solution.py:28
  40.8 0.6 broadcast_in_dim.4
  41.5 3.5 %all-to-all-start.1 = ((f32[16,1,128]{2,1,0:T(1,128)}), f32[16,1,128]{2,1,0:T(1,128)S(1)}, u32[]{:S(2)}, u32[]{:S(2)}) async-start(f32[16,1,128]{2,1,0:T(1,128)} %broadcast_in_dim.4), calls=%async_computation.1 | async-start | bytes 16384 | tf_op jit(solution)/shard_map/all_to_all | solution.py:34
  45.3 6.0 %all-to-all-done.1 = f32[16,1,128]{2,1,0:T(1,128)S(1)} async-done(((f32[16,1,128]{2,1,0:T(1,128)}), f32[16,1,128]{2,1,0:T(1,128)S(1)}, u32[]{:S(2)}, u32[]{:S(2)}) %all-to-all-start.1) | async-done | bytes 8224 | tf_op jit(solution)/shard_map/all_to_all | solution.py:34
  51.8 35.9 %all_to_all.31 = bf16[128,32,24]{0,2,1:T(8,128)(2,1)S(1)} all-to-all(bf16[128,32,24]{0,2,1:T(8,128)(2,1)S(1)} %bitcast.93), channel_id=1, replica_groups=mesh['sp'=32,'tp_0'=4,'tp_1'=4] {'sp'}, dimensions={1} | all-to-all | bytes 393216 | tf_op jit(solution)/shard_map/all_to_all | solution.py:133
  87.7 15.4 %all_gather.9 = bf16[512,768]{0,1:T(8,128)(2,1)} all-gather(bf16[128,768]{0,1:T(8,128)(2,1)S(1)} %bitcast.95), channel_id=1, replica_groups=mesh['sp'=32,'tp_0'=4,'tp_1'=4] {'tp_1'}, dimensions={0}, use_global_device_ids=true | all-gather | bytes 983040 | tf_op jit(solution)/shard_map/all_gather | solution.py:56
  103.2 37.7 %all-gather.3.cloned.1.call-done = bf16[2048,768]{0,1:T(8,128)(2,1)} async-done(((bf16[512,768]{0,1:T(8,128)(2,1)}), bf16[2048,768]{0,1:T(8,128)(2,1)}) %all-gather.3.cloned.1.call-update) | async-done | bytes 3145744 | tf_op jit(solution)/shard_map/all_gather | solution.py:56
  140.8 3.0 %convolution_bitcast_fusion.1 = f32[128,768]{0,1:T(8,128)S(1)} fusion(bf16[2048,768]{0,1:T(8,128)(2,1)} %all-gather.3.cloned.1.call-done, bf16[1,2048,128]{2,1,0:T(8,128)(2,1)S(1)} %copy-done.2), kind=kOutput, calls=%fused_computation.8 | convolution fusion | flops 402653184 | bytes 4063232 | tf_op jit(solution)/shard_map/dot_general | solution.py:61
  143.9 1.7 fusion.4
  145.7 15.9 %all_to_all.32 = bf16[16,128,128]{2,1,0:T(8,128)(2,1)S(1)} all-to-all(bf16[16,128,128]{2,1,0:T(8,128)(2,1)S(1)} %broadcast_in_dim.5), channel_id=1, replica_groups=mesh['sp'=32,'tp_0'=4,'tp_1'=4] {'tp_0','tp_1'}, dimensions={0} | all-to-all | bytes 1048576 | tf_op jit(solution)/shard_map/all_to_all | solution.py:34
  162.6 0.9 copy.105
  163.5 3.7 %all-to-all-start.3 = ((bf16[16,128,128]{1,2,0:T(8,128)(2,1)}), bf16[16,128,128]{1,2,0:T(8,128)(2,1)S(1)}, u32[]{:S(2)}, u32[]{:S(2)}) async-start(bf16[16,128,128]{1,2,0:T(8,128)(2,1)} %bitcast.89), calls=%async_computation.3 | async-start | bytes 1048576 | tf_op jit(solution)/shard_map/all_to_all | solution.py:28
  167.2 48.8 %all-gather.5.cloned.1.call-done = bf16[2048,768]{0,1:T(8,128)(2,1)} async-done(((bf16[128,768]{0,1:T(8,128)(2,1)}), bf16[2048,768]{0,1:T(8,128)(2,1)}) %all-gather.5.cloned.1.call-update) | async-done | bytes 3145744 | tf_op jit(solution)/shard_map/all_gather | solution.py:143
  216.0 3.6 %convolution_convert_fusion.2 = bf16[768,128]{1,0:T(8,128)(2,1)} fusion(bf16[2048,768]{0,1:T(8,128)(2,1)} %all-gather.5.cloned.1.call-done, bf16[1,2048,128]{2,1,0:T(8,128)(2,1)S(1)} %copy-done.10), kind=kOutput, calls=%fused_computation.11 | convolution fusion | flops 402751488 | bytes 3866624 | tf_op jit(solution)/shard_map/dot_general | solution.py:61
  219.6 14.4 %all-to-all-start.5 = ((bf16[128,32,24]{0,2,1:T(8,128)(2,1)}), bf16[128,32,24]{0,2,1:T(8,128)(2,1)S(1)}, u32[]{:S(2)}, u32[]{:S(2)}) async-start(bf16[128,32,24]{0,2,1:T(8,128)(2,1)} %bitcast.23), calls=%async_computation.5 | async-start | bytes 393216 | tf_op jit(solution)/shard_map/all_to_all | solution.py:146
  234.4 18.4 %all-to-all-done.5 = bf16[128,32,24]{0,2,1:T(8,128)(2,1)S(1)} async-done(((bf16[128,32,24]{0,2,1:T(8,128)(2,1)}), bf16[128,32,24]{0,2,1:T(8,128)(2,1)S(1)}, u32[]{:S(2)}, u32[]{:S(2)}) %all-to-all-start.5) | async-done | bytes 196640 | tf_op jit(solution)/shard_map/all_to_all | solution.py:146
  252.8 1.0 fusion.6
  (60 shorter events, 3.6 us)
Async XLA Ops:
  6.5 155.4 %copy-start = (bf16[128,2048]{1,0:T(8,128)(2,1)S(1)}, bf16[128,2048]{1,0:T(8,128)(2,1)}, u32[]{:S(2)}) copy-start(bf16[128,2048]{1,0:T(8,128)(2,1)} %param.33) | copy-start | bytes 1572868
  6.5 25.3 %copy-start.6 = (s32[128,4]{0,1:T(4,128)S(1)}, s32[128,4]{0,1:T(4,128)}, u32[]{:S(2)}) copy-start(s32[128,4]{0,1:T(4,128)} %param.26) | copy-start | bytes 6148
  6.5 34.3 %copy-start.5 = (bf16[128,128]{1,0:T(8,128)(2,1)S(1)}, bf16[128,128]{1,0:T(8,128)(2,1)}, u32[]{:S(2)}) copy-start(bf16[128,128]{1,0:T(8,128)(2,1)} %param.17) | copy-start | bytes 98308
  6.5 44.8 %copy-start.8 = (f32[128]{0:T(128)S(1)}, f32[128]{0:T(128)}, u32[]{:S(2)}) copy-start(f32[128]{0:T(128)} %param.25) | copy-start | bytes 1540
  7.3 10.3 %collective-permute-start.1 = (s32[2]{0:T(128)S(1)}, s32[2]{0:T(128)S(1)}, u32[]{:S(2)}, u32[]{:S(2)}) collective-permute-start(s32[2]{0:T(128)S(1)} %slice.51), channel_id=1, source_target_pairs={{0,16},{16,32},{32,48},{48,64},{64,80},{80,96},{96,112},{112,128},... | collective-permute-start | bytes 32 | tf_op jit(solution)/shard_map/ppermute | solution.py:18
  14.0 5.1 %collective-permute-start = (bf16[2,64,2]{1,2,0:T(2,128)(2,1)S(1)}, bf16[2,64,2]{1,2,0:T(2,128)(2,1)S(1)}, u32[]{:S(2)}, u32[]{:S(2)}) collective-permute-start(bf16[2,64,2]{1,2,0:T(2,128)(2,1)S(1)} %pad_maximum_fusion), channel_id=1, source_target_pairs={{0,16},{16,32},{32,48},{48,64},{64,80},{80,96},{96,112},{112,128},... | collective-permute-start | bytes 1544 | tf_op jit(solution)/shard_map/ppermute | solution.py:18
  22.4 118.5 %copy-start.2 = (bf16[1,2048,128]{2,1,0:T(8,128)(2,1)S(1)}, bf16[1,2048,128]{2,1,0:T(8,128)(2,1)}, u32[]{:S(2)}) copy-start(bf16[1,2048,128]{2,1,0:T(8,128)(2,1)} %param.28) | copy-start | bytes 1572868
  23.3 17.3 %all-to-all-start = ((bf16[16,128,128]{1,2,0:T(8,128)(2,1)}), bf16[16,128,128]{1,2,0:T(8,128)(2,1)S(1)}, u32[]{:S(2)}, u32[]{:S(2)}) async-start(bf16[16,128,128]{1,2,0:T(8,128)(2,1)} %bitcast.90), calls=%async_computation | async-start | bytes 1048576 | tf_op jit(solution)/shard_map/all_to_all | solution.py:28
  41.5 9.8 %all-to-all-start.1 = ((f32[16,1,128]{2,1,0:T(1,128)}), f32[16,1,128]{2,1,0:T(1,128)S(1)}, u32[]{:S(2)}, u32[]{:S(2)}) async-start(f32[16,1,128]{2,1,0:T(1,128)} %broadcast_in_dim.4), calls=%async_computation.1 | async-start | bytes 16384 | tf_op jit(solution)/shard_map/all_to_all | solution.py:34
  44.9 95.9 %all-gather.3.cloned.1.call-start = ((), (), s32[]{:S(2)}) async-start(), calls=%async_computation.6 | async-start | bytes 3932160 | tf_op jit(solution)/shard_map/all_gather | solution.py:56
  103.1 40.8 %copy-start.9 = (bf16[1,2048,128]{2,1,0:T(8,128)(2,1)S(1)}, bf16[1,2048,128]{2,1,0:T(8,128)(2,1)}, u32[]{:S(2)}) copy-start(bf16[1,2048,128]{2,1,0:T(8,128)(2,1)} %param.29) | copy-start | bytes 1572868
  103.1 112.9 %all-gather.5.cloned.1.call-start = ((), (), s32[]{:S(2)}) async-start(), calls=%async_computation.7 | async-start | bytes 3342336 | tf_op jit(solution)/shard_map/all_gather | solution.py:143
  140.8 3.0 %copy-start.1 = (bf16[2048,768]{0,1:T(8,128)(2,1)S(1)}, bf16[2048,768]{0,1:T(8,128)(2,1)}, u32[]{:S(2)}) copy-start(bf16[2048,768]{0,1:T(8,128)(2,1)} %all-gather.3.cloned.1.call-done) | copy-start | bytes 9437188
  143.9 17.7 %copy-start.3 = (bf16[2048,128]{1,0:T(8,128)(2,1)S(1)}, bf16[2048,128]{1,0:T(8,128)(2,1)}, u32[]{:S(2)}) copy-start(bf16[2048,128]{1,0:T(8,128)(2,1)} %param.31) | copy-start | bytes 1572868
  145.6 16.4 %copy-start.4 = (bf16[2048,128]{1,0:T(8,128)(2,1)S(1)}, bf16[2048,128]{1,0:T(8,128)(2,1)}, u32[]{:S(2)}) copy-start(bf16[2048,128]{1,0:T(8,128)(2,1)} %param.32) | copy-start | bytes 1572868
  145.7 70.4 %copy-start.10 = (bf16[1,2048,128]{2,1,0:T(8,128)(2,1)S(1)}, bf16[1,2048,128]{2,1,0:T(8,128)(2,1)}, u32[]{:S(2)}) copy-start(bf16[1,2048,128]{2,1,0:T(8,128)(2,1)} %param.30) | copy-start | bytes 1572868
  163.5 70.5 %copy-start.7 = (f32[128,4]{0,1:T(4,128)S(1)}, f32[128,4]{0,1:T(4,128)}, u32[]{:S(2)}) copy-start(f32[128,4]{0,1:T(4,128)} %param.27) | copy-start | bytes 6148
  163.5 56.1 %all-to-all-start.3 = ((bf16[16,128,128]{1,2,0:T(8,128)(2,1)}), bf16[16,128,128]{1,2,0:T(8,128)(2,1)S(1)}, u32[]{:S(2)}, u32[]{:S(2)}) async-start(bf16[16,128,128]{1,2,0:T(8,128)(2,1)} %bitcast.89), calls=%async_computation.3 | async-start | bytes 1048576 | tf_op jit(solution)/shard_map/all_to_all | solution.py:28
  219.6 33.2 %all-to-all-start.5 = ((bf16[128,32,24]{0,2,1:T(8,128)(2,1)}), bf16[128,32,24]{0,2,1:T(8,128)(2,1)S(1)}, u32[]{:S(2)}, u32[]{:S(2)}) async-start(bf16[128,32,24]{0,2,1:T(8,128)(2,1)} %bitcast.23), calls=%async_computation.5 | async-start | bytes 393216 | tf_op jit(solution)/shard_map/all_to_all | solution.py:146
Sparse Core Ops, SparseCore 0:
  103.2 37.5 all-gather.2
  145.7 70.2 all-gather.4
where the time goes:
time: 262 us; the launch traced here: 261 us
  waiting for transfers between devices  120 us (46%)
  blocking collectives  67.2 us (26%)
  starting transfers between devices  35.2 us (13%)
  between operations  13.7 us (5%)
  matrix products  11.7 us (4%)
  local copies, waits for them, and re-layouts  7.81 us (3%)
  other arithmetic  5.27 us (2%)
    all_gather x1, waiting for transfers between devices, local(): lax.all_gather(expert_mid, TP, axis=0, tiled=True)  48.8 us
    all_gather x1, waiting for transfers between devices, gather_axes(): nearer = lax.all_gather(x, axes[-1], axis=dim, tiled=True)  37.7 us
    all_to_all x1, blocking collectives, local(): lax.all_to_all(sent.reshape(feat_rows, sp_count, capacity), 'sp', split_a...  35.9 us
    all_to_all x1, waiting for transfers between devices, local(): lax.all_to_all(summed.reshape(feat_rows, sp_count, capacity), 'sp', split...  18.4 us
    all_to_all x1, blocking collectives, from_everyone(): lax.all_to_all(jnp.broadcast_to(x[None], (size, *x.shape)), axis, 0, 0, t...  15.9 us
    all_gather x1, blocking collectives, gather_axes(): nearer = lax.all_gather(x, axes[-1], axis=dim, tiled=True)  15.4 us
    all_to_all x1, starting transfers between devices, local(): lax.all_to_all(summed.reshape(feat_rows, sp_count, capacity), 'sp', split...  14.4 us
    dot_general x6, matrix products, contract_rows(): lax.dot_general(left, right, (((0,), (0,)), ((), ())), preferred_element_...  10.5 us
  transfers between devices with their start and end apart: 8, of which 5 were waited for; matrix products, arithmetic and copies ran while one was open for 5% of the time, Pallas kernels for 0%

commit v1 on v0

v1 whole, which is shorter than its diff:
```python
import jax
import jax.numpy as jnp
from jax import lax
from jax.experimental import pallas as pl
from jax.experimental.pallas import tpu as pltpu
from jax.sharding import PartitionSpec as P

F32 = jnp.float32
BF16 = jnp.bfloat16
MESH = pl.DeviceIdType.MESH
EPS = 1e-06

D = 2048
T = 128
HEAD = 64
N_SP = 32
N_TP = 16
N_Z = 16
SIDE = 4
CAP = 24
TOP_K = 4
SLOTS = N_SP * CAP
CHUNKS = 2
PER_CHUNK = N_SP // CHUNKS
HALF = PER_CHUNK // 2
QUARTER = HALF // 2
NEAR = 3


def dot(a, b, contract=((1,), (0,)), precision=None):
    return lax.dot_general(
        a, b, (contract, ((), ())), precision=precision, preferred_element_type=F32
    )


def iota(shape, dim):
    return lax.broadcasted_iota(jnp.int32, shape, dim)


def column_of(row, n):
    eye = iota((n, n), 0) == iota((n, n), 1)
    return jnp.sum(jnp.where(eye, jnp.broadcast_to(row, (n, n)), 0.0), axis=1, keepdims=True)


def kernel(
    stream,
    values_in,
    in_gate,
    out_gate,
    documents,
    conv_taps,
    head_gain,
    mix_weight,
    norm_gain,
    routes,
    route_weight,
    expert_gate,
    expert_up,
    expert_down,
    shared_gate,
    shared_up,
    shared_down,
    out,
    halo_v,
    halo_g,
    halo_d,
    mix_w,
    w_gu,
    w_down,
    s_gu,
    s_down,
    mix_part,
    mix_in,
    sq_out,
    sq_in,
    normed_all,
    pick,
    comb_hi,
    comb_lo,
    disp_out,
    rows_all,
    mid_all,
    ret_out,
    ret_in,
    sh_part,
    sh_in,
    hidden,
    load_sem,
    halo_s,
    halo_r,
    mix_s,
    mix_r,
    sq_s,
    sq_r,
    nrm_s,
    nrm_r,
    disp_s,
    disp_r,
    gat_s,
    gat_r,
    ret_s,
    ret_r,
    sh_s,
    sh_r,
):
    sp = lax.axis_index("sp")
    tp = lax.axis_index("tp")
    z, core = sp // 2, sp % 2
    y, x = tp // SIDE, tp % SIDE

    def remote(src, dst, send, recv, **where):
        return pltpu.make_async_remote_copy(
            src_ref=src,
            dst_ref=dst,
            send_sem=send,
            recv_sem=recv,
            device_id=where,
            device_id_type=MESH,
        )

    barrier = pltpu.get_barrier_semaphore()

    @pl.loop(1, N_SP)
    def _(step):
        pl.semaphore_signal(
            barrier, inc=1, device_id={"sp": (sp + step) % N_SP}, device_id_type=MESH
        )

    @pl.loop(1, N_TP)
    def _(step):
        pl.semaphore_signal(
            barrier, inc=1, device_id={"tp": (tp + step) % N_TP}, device_id_type=MESH
        )

    loads = [
        pltpu.make_async_copy(src, dst, load_sem.at[i])
        for i, (src, dst) in enumerate(
            [
                (mix_weight, mix_w),
                (shared_gate, s_gu.at[:, pl.ds(0, T)]),
                (shared_up, s_gu.at[:, pl.ds(T, T)]),
                (shared_down, s_down),
                (expert_gate.at[0], w_gu.at[:, pl.ds(0, T)]),
                (expert_up.at[0], w_gu.at[:, pl.ds(T, T)]),
                (expert_down.at[0], w_down),
            ]
        )
    ]
    for load in loads:
        load.start()

    lane = iota((T, T), 1)
    named = jnp.zeros((T, T), F32)
    weight = jnp.zeros((T, T), F32)
    for k in range(TOP_K):
        hit = routes[:, k : k + 1] == lane
        named = jnp.where(hit, 1.0, named)
        weight = jnp.where(hit, route_weight[:, k : k + 1], weight)
    before = jnp.where(iota((T, T), 0) > lane, 1.0, 0.0).astype(BF16)
    earlier = dot(before, named.astype(BF16))
    slot = jnp.where(named > 0, earlier, 200.0).astype(BF16)

    def slot_number(shape, dim):
        number = iota(shape, dim).astype(F32)
        return number - CAP * jnp.floor((number + 0.5) * (1.0 / CAP))

    away = iota((SLOTS, T), 0) - CAP * iota((SLOTS, T), 1)
    owner = jnp.where((away >= 0) & (away < CAP), 1.0, 0.0).astype(BF16)
    taken = dot(owner, slot, ((1,), (1,)))
    pick[...] = jnp.where(taken == slot_number((SLOTS, T), 0), 1.0, 0.0).astype(BF16)
    away = iota((T, SLOTS), 1) - CAP * iota((T, SLOTS), 0)
    owner = jnp.where((away >= 0) & (away < CAP), 1.0, 0.0).astype(BF16)
    taken = dot(slot, owner) == slot_number((T, SLOTS), 1)
    weight_hi = weight.astype(BF16)
    weight_lo = (weight - weight_hi.astype(F32)).astype(BF16)
    comb_hi[...] = jnp.where(taken, dot(weight_hi, owner), 0.0).astype(BF16)
    comb_lo[...] = jnp.where(taken, dot(weight_lo, owner), 0.0).astype(BF16)

    pl.semaphore_wait(barrier, N_SP + N_TP - 2)

    behind = (sp + 1) % N_SP
    halos = [
        remote(src, dst, halo_s.at[i], halo_r.at[i], sp=behind)
        for i, (src, dst) in enumerate(
            [(values_in, halo_v), (in_gate, halo_g), (documents, halo_d)]
        )
    ]
    for halo in halos:
        halo.start()
    product = values_in[...].astype(F32) * in_gate[...].astype(F32)
    docs = jnp.broadcast_to(documents[...], (8, T))
    tap = [column_of(conv_taps[j : j + 1, :], HEAD) for j in range(3)]
    gain_col = column_of(head_gain[...], HEAD)
    for halo in halos:
        halo.wait_recv()
    product_before = halo_v[...].astype(F32) * halo_g[...].astype(F32)
    docs_before = jnp.where(sp == 0, -1, jnp.broadcast_to(halo_d[...], (8, T)))
    convolved = jnp.zeros((HEAD, T), F32)
    for j in range(3):
        back = 2 - j
        if back:
            shifted = jnp.where(
                iota((HEAD, T), 1) < back,
                pltpu.roll(product_before, back, 1),
                pltpu.roll(product, back, 1),
            )
            docs_then = jnp.where(
                iota((8, T), 1) < back,
                pltpu.roll(docs_before, back, 1),
                pltpu.roll(docs, back, 1),
            )
            same = jnp.where(docs_then == docs, 1.0, 0.0)[0:1, :]
            convolved = convolved + tap[j] * shifted * same
        else:
            convolved = convolved + tap[j] * product
    mixed = out_gate[...].astype(F32) * convolved
    spread = jnp.mean(mixed * mixed, axis=0, keepdims=True)
    heads = (mixed * lax.rsqrt(spread + EPS) * gain_col).T.astype(BF16)

    loads[0].wait()
    for j in range(N_TP // 2):
        part = dot(heads, mix_w[:, 2 * T * j : 2 * T * (j + 1)]).astype(BF16)
        mix_part[2 * j] = part[:, :T]
        mix_part[2 * j + 1] = part[:, T:]

    def to_plane(src_of, dst, send, recv):
        def copy(step):
            peer = (tp + step) % N_TP
            return remote(src_of(peer), dst.at[tp], send.at[step], recv.at[step], tp=peer)

        return copy

    def start_plane(copy):
        @pl.loop(1, N_TP)
        def _(step):
            copy(step).start()

    def wait_plane(copy):
        @pl.loop(1, N_TP)
        def _(step):
            copy(step).wait_recv()

    mix_copy = to_plane(lambda peer: mix_part.at[peer], mix_in, mix_s, mix_r)
    start_plane(mix_copy)
    mix_in[tp] = mix_part[tp]
    total = stream[...].astype(F32).T
    wait_plane(mix_copy)
    for j in range(N_TP):
        total = total + mix_in[j].astype(F32)
    hidden[...] = total

    squares = dot(jnp.ones((8, T), F32), total * total, ((1,), (1,)), lax.Precision.HIGHEST)
    sq_out[...] = squares
    sq_copy = to_plane(lambda peer: sq_out, sq_in, sq_s, sq_r)
    start_plane(sq_copy)
    sq_in[tp] = squares
    wait_plane(sq_copy)
    squares = sq_in[0]
    for j in range(1, N_TP):
        squares = squares + sq_in[j]
    scale = column_of(lax.rsqrt(squares / D + EPS)[0:1, :], T)
    normed = (hidden[...] * scale * norm_gain[...]).astype(BF16)

    normed_all[tp] = normed
    disp_out[...] = dot(pick[...], normed).astype(BF16).reshape(N_SP, CAP, T)
    shifts = [0] + [s for d in range(1, 8) for s in (d, -d)] + [8]
    order = [(dz, other) for dz in shifts for other in (0, 1)][1:]

    def disp_copy(dz, other):
        place = (dz + NEAR) % N_Z
        expert = 2 * ((z - dz + N_Z) % N_Z) + ((core + 1 + other) % 2 if dz else 1 - core)
        block = 2 * place + core
        return remote(
            disp_out.at[expert],
            rows_all.at[y, x, block],
            disp_s.at[2 * place + other],
            disp_r.at[block],
            sp=expert,
        )

    def arrived(dz, other):
        place = (dz + NEAR) % N_Z
        return 2 * place + (other if dz else 1 - core)

    for dz, other in order:
        disp_copy(dz, other).start()
    own = 2 * NEAR + core
    rows_all[y, x, own] = disp_out[sp]

    nrm_copy = to_plane(lambda peer: normed_all.at[tp], normed_all, nrm_s, nrm_r)
    start_plane(nrm_copy)

    def wait_disp(chunk):
        for dz, other in order:
            if ((dz + NEAR) % N_Z) // (N_Z // CHUNKS) == chunk:
                block = arrived(dz, other)
                remote(
                    disp_out.at[0], rows_all.at[y, x, block], disp_s.at[0], disp_r.at[block], sp=behind
                ).wait_recv()

    def tp_at(axis, way):
        if axis == 0:
            return SIDE * y + (x + way + SIDE) % SIDE
        return SIDE * ((y + way + SIDE) % SIDE) + x

    def gather_copies(buf, which, chunk, step):
        copies = []
        for half in range(2):
            start = PER_CHUNK * chunk + HALF * half
            axis = half if step < 2 else 1 - half
            for way in (1, -1):
                quarter = pl.ds(start if way > 0 else start + QUARTER, QUARTER)
                whole = pl.ds(start, HALF)
                from_x = (x - way + SIDE) % SIDE
                from_y = (y - way + SIDE) % SIDE
                if step == 0:
                    ref = buf.at[y, x, whole]
                elif step == 1:
                    ref = buf.at[y, from_x, quarter] if axis == 0 else buf.at[from_y, x, quarter]
                elif step == 2:
                    ref = buf.at[:, x, whole] if axis == 0 else buf.at[y, :, whole]
                else:
                    ref = buf.at[:, from_x, quarter] if axis == 0 else buf.at[from_y, :, quarter]
                index = (((which * CHUNKS + chunk) * 4 + step) * 2 + half) * 2 + (way > 0)
                copies.append(
                    remote(ref, ref, gat_s.at[index], gat_r.at[index], tp=tp_at(axis, way))
                )
        return copies

    bufs = (rows_all, mid_all)

    def go(which, chunk, step):
        for copy in gather_copies(bufs[which], which, chunk, step):
            copy.start()

    def got(which, chunk, step):
        for copy in gather_copies(bufs[which], which, chunk, step):
            copy.wait_recv()

    def gathered(buf, chunk):
        part = pl.ds(PER_CHUNK * chunk, PER_CHUNK)
        return jnp.concatenate(
            [
                buf[i, j, part].reshape(PER_CHUNK * CAP, T)
                for i in range(SIDE)
                for j in range(SIDE)
            ],
            axis=1,
        )

    def silu(v):
        return v / (1.0 + jnp.exp(-v))

    def gate_up(chunk):
        both = dot(gathered(rows_all, chunk), w_gu[...])
        mid = (silu(both[:, :T]) * both[:, T:]).astype(BF16)
        mid_all[y, x, pl.ds(PER_CHUNK * chunk, PER_CHUNK)] = mid.reshape(PER_CHUNK, CAP, T)

    def down(chunk):
        result = dot(gathered(mid_all, chunk), w_down[...]).astype(BF16)
        ret_out[pl.ds(PER_CHUNK * chunk, PER_CHUNK)] = result.reshape(PER_CHUNK, CAP, T)

    def ret_copy(dz, other):
        place = (dz + NEAR) % N_Z
        group_core = (core + 1 + other) % 2 if dz else 1 - core
        group = 2 * ((z + dz + N_Z) % N_Z) + group_core
        return remote(
            ret_out.at[2 * place + group_core],
            ret_in.at[sp],
            ret_s.at[2 * place + other],
            ret_r.at[2 * place + core],
            sp=group,
        )

    def start_ret(chunk):
        for dz, other in order[::-1]:
            if ((dz + NEAR) % N_Z) // (N_Z // CHUNKS) == chunk:
                ret_copy(dz, other).start()

    def shared_expert():
        for load in loads[1:4]:
            load.wait()
        everything = jnp.concatenate([normed_all[j] for j in range(N_TP)], axis=1)
        both = dot(everything, s_gu[...])
        mid = (silu(both[:, :T]) * both[:, T:]).astype(BF16)
        for j in range(N_TP // 2):
            part = dot(mid, s_down[:, 2 * T * j : 2 * T * (j + 1)]).astype(BF16)
            sh_part[2 * j] = part[:, :T]
            sh_part[2 * j + 1] = part[:, T:]

    sh_copy = to_plane(lambda peer: sh_part.at[peer], sh_in, sh_s, sh_r)

    wait_disp(0)
    go(0, 0, 0)
    got(0, 0, 0)
    go(0, 0, 1)
    wait_plane(nrm_copy)
    shared_expert()
    sh_in[tp] = sh_part[tp]
    got(0, 0, 1)
    go(0, 0, 2)
    wait_disp(1)
    go(0, 1, 0)
    got(0, 1, 0)
    go(0, 1, 1)
    got(0, 0, 2)
    go(0, 0, 3)
    got(0, 1, 1)
    go(0, 1, 2)
    for load in loads[4:]:
        load.wait()
    got(0, 0, 3)
    gate_up(0)
    go(1, 0, 0)
    got(0, 1, 2)
    go(0, 1, 3)
    got(1, 0, 0)
    go(1, 0, 1)
    got(0, 1, 3)
    gate_up(1)
    go(1, 1, 0)
    got(1, 0, 1)
    go(1, 0, 2)
    got(1, 1, 0)
    go(1, 1, 1)
    got(1, 0, 2)
    go(1, 0, 3)
    got(1, 1, 1)
    go(1, 1, 2)
    got(1, 0, 3)
    down(0)
    start_ret(0)
    ret_in[sp] = ret_out[own]
    got(1, 1, 2)
    go(1, 1, 3)
    start_plane(sh_copy)
    got(1, 1, 3)
    down(1)
    start_ret(1)

    wait_plane(sh_copy)
    total = hidden[...]
    for j in range(N_TP):
        total = total + sh_in[j].astype(F32)
    for dz, other in order:
        block = arrived(dz, other)
        remote(ret_out.at[0], ret_in.at[0], ret_s.at[0], ret_r.at[block], sp=behind).wait_recv()
    returned = ret_in[...].reshape(SLOTS, T)
    total = total + dot(comb_hi[...], returned) + dot(comb_lo[...], returned)
    out[...] = total.T.astype(BF16)

    for halo in halos:
        halo.wait_send()
    for copy in (mix_copy, sq_copy, nrm_copy, sh_copy):

        @pl.loop(1, N_TP)
        def _(step, copy=copy):
            copy(step).wait_send()

    for dz, other in order:
        disp_copy(dz, other).wait_send()
        ret_copy(dz, other).wait_send()
    for which in range(2):
        for chunk in range(CHUNKS):
            for step in range(4):
                for copy in gather_copies(bufs[which], which, chunk, step):
                    copy.wait_send()


def local(
    stream,
    values_in,
    in_gate,
    out_gate,
    documents,
    conv_taps,
    head_gain,
    mix_weight,
    norm_gain,
    routes,
    route_weight,
    expert_gate,
    expert_up,
    expert_down,
    shared_gate,
    shared_up,
    shared_down,
):
    vmem = pl.BlockSpec(memory_space=pltpu.VMEM)
    hbm = pl.BlockSpec(memory_space=pl.ANY)
    dma = pltpu.SemaphoreType.DMA
    gathers = 2 * CHUNKS * 4 * 4
    return pl.pallas_call(
        kernel,
        name="layer",
        out_shape=jax.ShapeDtypeStruct((T, T), BF16),
        in_specs=[vmem] * 7 + [hbm] + [vmem] * 3 + [hbm] * 6,
        out_specs=vmem,
        scratch_shapes=[
            pltpu.VMEM((HEAD, T), BF16),
            pltpu.VMEM((HEAD, T), BF16),
            pltpu.VMEM((1, T), jnp.int32),
            pltpu.VMEM((HEAD, D), BF16),
            pltpu.VMEM((D, 2 * T), BF16),
            pltpu.VMEM((D, T), BF16),
            pltpu.VMEM((D, 2 * T), BF16),
            pltpu.VMEM((T, D), BF16),
            pltpu.VMEM((N_TP, T, T), BF16),
            pltpu.VMEM((N_TP, T, T), BF16),
            pltpu.VMEM((8, T), F32),
            pltpu.VMEM((N_TP, 8, T), F32),
            pltpu.VMEM((N_TP, T, T), BF16),
            pltpu.VMEM((SLOTS, T), BF16),
            pltpu.VMEM((T, SLOTS), BF16),
            pltpu.VMEM((T, SLOTS), BF16),
            pltpu.VMEM((N_SP, CAP, T), BF16),
            pltpu.VMEM((SIDE, SIDE, N_SP, CAP, T), BF16),
            pltpu.VMEM((SIDE, SIDE, N_SP, CAP, T), BF16),
            pltpu.VMEM((N_SP, CAP, T), BF16),
            pltpu.VMEM((N_SP, CAP, T), BF16),
            pltpu.VMEM((N_TP, T, T), BF16),
            pltpu.VMEM((N_TP, T, T), BF16),
            pltpu.VMEM((T, T), F32),
            dma((7,)),
            dma((3,)),
            dma((3,)),
            dma((N_TP,)),
            dma((N_TP,)),
            dma((N_TP,)),
            dma((N_TP,)),
            dma((N_TP,)),
            dma((N_TP,)),
            dma((N_SP,)),
            dma((N_SP,)),
            dma((gathers,)),
            dma((gathers,)),
            dma((N_SP,)),
            dma((N_SP,)),
            dma((N_TP,)),
            dma((N_TP,)),
        ],
        compiler_params=pltpu.CompilerParams(collective_id=0, has_side_effects=True),
    )(
        stream,
        values_in,
        in_gate,
        out_gate,
        documents[None, :],
        conv_taps,
        head_gain[None, :],
        mix_weight,
        norm_gain[None, :],
        routes,
        route_weight,
        expert_gate,
        expert_up,
        expert_down,
        shared_gate,
        shared_up,
        shared_down,
    )


def solution(mesh):
    in_specs = (
        P("tp", "sp"),
        P("tp", "sp"),
        P("tp", "sp"),
        P("tp", "sp"),
        P("sp"),
        P(None, "tp"),
        P("tp"),
        P("tp", None),
        P("tp"),
        P("sp", None),
        P("sp", None),
        P("sp", None, "tp"),
        P("sp", None, "tp"),
        P("sp", None, "tp"),
        P(None, "tp"),
        P(None, "tp"),
        P("tp", None),
    )
    return jax.shard_map(
        local, mesh=mesh, in_specs=in_specs, out_specs=P("tp", "sp"), check_vma=False
    )
```

time: 262 us -> 109 us (0.42)
  waiting for transfers between devices: 120 us -> 0 us
  Pallas kernels: 0 us -> 105 us
  blocking collectives: 67.2 us -> 0 us
  starting transfers between devices: 35.2 us -> 0 us
  between operations: 13.7 us -> 0.01 us
  matrix products: 11.7 us -> 0 us
  other arithmetic: 5.27 us -> 0 us
  local copies, waits for them, and re-layouts: 7.81 us -> 3.51 us
    pallas_call x0 -> x1, Pallas kernels: none -> 105 us  [local(): pl.pallas_call(kernel, name='layer', out_shape=jax.ShapeDtypeStruct((T, T...]
    all_gather x2 -> x0, waiting for transfers between devices: 86.5 us -> none  [the longest x1 48.8 us: local(): lax.all_gather(expert_mid, TP, axis=0, tiled=True)]
    all_to_all x2 -> x0, blocking collectives: 51.8 us -> none  [the longest x1 35.9 us: local(): lax.all_to_all(sent.reshape(feat_rows, sp_count, capacity), 'sp', split_a...]
    all_to_all x4 -> x0, waiting for transfers between devices: 33.1 us -> none  [the longest x1 18.4 us: local(): lax.all_to_all(summed.reshape(feat_rows, sp_count, capacity), 'sp', split...]
    all_to_all x4 -> x0, starting transfers between devices: 28.3 us -> none  [the longest x1 14.4 us: local(): lax.all_to_all(summed.reshape(feat_rows, sp_count, capacity), 'sp', split...]
    all_gather x1 -> x0, blocking collectives: 15.4 us -> none  [gather_axes(): nearer = lax.all_gather(x, axes[-1], axis=dim, tiled=True)]
    dot_general x8 -> x0, matrix products: 11.7 us -> none  [the longest x6 10.5 us: contract_rows(): lax.dot_general(left, right, (((0,), (0,)), ((), ())), preferred_element_...]
    ppermute x2 -> x0, starting transfers between devices: 6.83 us -> none  [from_behind(): return lax.ppermute(x, axis, pairs)]
  transfers between devices with their start and end apart: 8 -> 0, of which waited for: 5 -> 0; matrix products, arithmetic and copies ran while one was open for 5% -> 0% of each run, Pallas kernels for 0% -> 0%
where the time goes in v1:
time: 109 us; the launch traced here: 108 us
  Pallas kernels  105 us (96%)
  local copies, waits for them, and re-layouts  3.51 us (3%)
    pallas_call x1, Pallas kernels, local(): pl.pallas_call(kernel, name='layer', out_shape=jax.ShapeDtypeStruct((T, T...  105 us
    unnamed x7, local copies, waits for them, and re-layouts  3.51 us

profile of v1, /device:TPU:1, one launch (start us, length us, event | category | flops | bytes accessed | tf_op | source)
XLA Modules:
  0.0 108.2 jit_solution(18260152063366800777)
XLA Ops:
  0.0 0.0 copy-start
  0.0 0.7 copy-done
  0.7 0.0 copy-start.1
  0.7 0.7 copy.18.routes
  1.4 0.0 copy-done.1
  1.4 0.7 copy.19.route_weight
  2.1 104.6 %layer.1 = bf16[128,128]{1,0:T(8,128)(2,1)} custom-call(bf16[128,128]{1,0:T(8,128)(2,1)} %stream.1, bf16[64,128]{1,0:T(8,128)(2,1)} %values_in.1, bf16[64,128]{1,0:T(8,128)(2,1)} %in_gate.1, bf16[64,128]{1,0:T(8,128)(2,1)} %out_gate.1, s32[1,128]{1,0:T(1,128)} %bitcast.3, f32[3,64]{1,0:T(4,128)} %conv_taps.1, f32[1,64]{1,0:T(1,128)} %bitcast.4, ...), custom_call_target="tpu_custom_call" | custom-call | tf_op jit(solution)/shard_map/layer/pallas_call | solution.py:493
  106.8 1.4 %copy.21 = bf16[128,128]{1,0:T(8,128)(2,1)} copy(bf16[128,128]{1,0:T(8,128)(2,1)} %layer.1) | data formatting | bytes 65536
Async XLA Ops:
  0.0 0.7 copy-start
  0.7 0.7 copy-start.1

commit v2 on v1

v2 whole, which is shorter than its diff:
```python
import jax
import jax.numpy as jnp
from jax import lax
from jax.experimental import pallas as pl
from jax.experimental.pallas import tpu as pltpu
from jax.sharding import PartitionSpec as P

F32 = jnp.float32
BF16 = jnp.bfloat16
MESH = pl.DeviceIdType.MESH
EPS = 1e-06

D = 2048
T = 128
HEAD = 64
N_SP = 32
N_TP = 16
N_Z = 16
SIDE = 4
CAP = 24
TOP_K = 4
SLOTS = N_SP * CAP
DISTANCES = ((0, 1, -1, 2), (8, -7, 7, -6, 6, -5, 5, -4), (4, -3, 3, -2))
PLACES = [dz for chunk in DISTANCES for dz in chunk]
CHUNKS = len(DISTANCES)
SIZES = [2 * len(chunk) for chunk in DISTANCES]
STARTS = [sum(SIZES[:c]) for c in range(CHUNKS)]
STAGES = 9
GATHER = (4, 12, 8, 2)
EXPERT = (4, 4, 8, 4)
COPIES = sum(GATHER) + sum(EXPERT)
ALL = COPIES * CHUNKS + sum(GATHER)
LAG = 1.01
SHARED = {1: (0, 1), 2: (0, 2), 3: (0, 3), 4: (1, 3)}
SHARED_SEND_AFTER = (CHUNKS - 1, 7)


def dot(a, b, contract=((1,), (0,)), precision=None):
    return lax.dot_general(
        a, b, (contract, ((), ())), precision=precision, preferred_element_type=F32
    )


def iota(shape, dim):
    return lax.broadcasted_iota(jnp.int32, shape, dim)


def column_of(row, n):
    eye = iota((n, n), 0) == iota((n, n), 1)
    return jnp.sum(jnp.where(eye, jnp.broadcast_to(row, (n, n)), 0.0), axis=1, keepdims=True)


def kernel(
    stream,
    values_in,
    in_gate,
    out_gate,
    documents,
    conv_taps,
    head_gain,
    mix_weight,
    norm_gain,
    routes,
    route_weight,
    expert_gate,
    expert_up,
    expert_down,
    shared_gate,
    shared_up,
    shared_down,
    out,
    halo_v,
    halo_g,
    halo_d,
    mix_here,
    mix_w,
    w_gu,
    w_down,
    w_one,
    w_two,
    s_gu,
    s_down,
    head_all,
    gains,
    normed_all,
    pick,
    comb_hi,
    comb_lo,
    disp_out,
    rows_all,
    mid_all,
    part,
    direct,
    chain,
    chain_out,
    final,
    ret_out,
    ret_in,
    sh_part,
    sh_in,
    hidden,
    load_sem,
    down_s,
    down_r,
    halo_s,
    halo_r,
    mix_s,
    mix_r,
    swap_s,
    swap_r,
    head_s,
    head_r,
    gain_s,
    gain_r,
    nrm_s,
    nrm_r,
    disp_s,
    disp_r,
    gat_s,
    gat_r,
    ret_s,
    ret_r,
    sh_s,
    sh_r,
):
    sp = lax.axis_index("sp")
    tp = lax.axis_index("tp")
    z, core = sp // 2, sp % 2
    y, x = tp // SIDE, tp % SIDE

    def remote(src, dst, send, recv, **where):
        return pltpu.make_async_remote_copy(
            src_ref=src,
            dst_ref=dst,
            send_sem=send,
            recv_sem=recv,
            device_id=where,
            device_id_type=MESH,
        )

    barrier = pltpu.get_barrier_semaphore()

    @pl.loop(1, N_SP)
    def _(step):
        pl.semaphore_signal(
            barrier, inc=1, device_id={"sp": (sp + step) % N_SP}, device_id_type=MESH
        )

    @pl.loop(1, N_TP)
    def _(step):
        pl.semaphore_signal(
            barrier, inc=1, device_id={"tp": (tp + step) % N_TP}, device_id_type=MESH
        )

    loads = [
        pltpu.make_async_copy(src, dst, load_sem.at[i])
        for i, (src, dst) in enumerate(
            [
                (mix_weight, mix_here),
                (expert_down, w_down),
                (expert_down.at[y], w_one.at[y]),
                (expert_down.at[:, x], w_two.at[x]),
                (shared_gate, s_gu.at[:, pl.ds(0, T)]),
                (shared_up, s_gu.at[:, pl.ds(T, T)]),
                (shared_down, s_down),
                (expert_gate.at[0], w_gu.at[:, pl.ds(0, T)]),
                (expert_up.at[0], w_gu.at[:, pl.ds(T, T)]),
            ]
        )
    ]
    for load in loads:
        load.start()

    line = iota((T, T), 0)
    named = jnp.zeros((T, T), F32)
    weight = jnp.zeros((T, T), F32)
    for k in range(TOP_K):
        hit = routes[k : k + 1, :] == line
        named = jnp.where(hit, 1.0, named)
        weight = jnp.where(hit, route_weight[k : k + 1, :], weight)
    before = jnp.where(line < iota((T, T), 1), 1.0, 0.0).astype(BF16)
    earlier = dot(named.astype(BF16), before)
    slot = jnp.where(named > 0, earlier, 200.0)
    slot_t = slot.T.astype(BF16)
    slot = slot.astype(BF16)
    weight = weight.T

    def slot_number(shape, dim):
        number = iota(shape, dim).astype(F32)
        return number - CAP * jnp.floor((number + 0.5) * (1.0 / CAP))

    away = iota((SLOTS, T), 0) - CAP * iota((SLOTS, T), 1)
    owner = jnp.where((away >= 0) & (away < CAP), 1.0, 0.0).astype(BF16)
    taken = dot(owner, slot)
    pick[...] = jnp.where(taken == slot_number((SLOTS, T), 0), 1.0, 0.0).astype(BF16)
    away = iota((T, SLOTS), 1) - CAP * iota((T, SLOTS), 0)
    owner = jnp.where((away >= 0) & (away < CAP), 1.0, 0.0).astype(BF16)
    taken = dot(slot_t, owner) == slot_number((T, SLOTS), 1)
    weight_hi = weight.astype(BF16)
    weight_lo = (weight - weight_hi.astype(F32)).astype(BF16)
    comb_hi[...] = jnp.where(taken, dot(weight_hi, owner), 0.0).astype(BF16)
    comb_lo[...] = jnp.where(taken, dot(weight_lo, owner), 0.0).astype(BF16)

    pl.semaphore_wait(barrier, N_SP + N_TP - 2)

    behind = (sp + 1) % N_SP
    halos = [
        remote(src, dst, halo_s.at[i], halo_r.at[i], sp=behind)
        for i, (src, dst) in enumerate(
            [(values_in, halo_v), (in_gate, halo_g), (documents, halo_d)]
        )
    ]
    for halo in halos:
        halo.start()

    def to_plane(src_of, dst, send, recv):
        def copy(step):
            peer = (tp + step) % N_TP
            return remote(src_of(peer), dst, send.at[step], recv.at[step], tp=peer)

        return copy

    def start_plane(copy):
        @pl.loop(1, N_TP)
        def _(step):
            copy(step).start()

    def wait_plane(copy):
        @pl.loop(1, N_TP)
        def _(step):
            copy(step).wait_recv()

    rows = pl.ds(core * (HEAD // 2), HEAD // 2)

    def columns(peer):
        return mix_here.at[rows, pl.ds(pl.multiple_of(peer * T, T), T)]

    mix_copy = to_plane(columns, mix_w.at[core, tp], mix_s, mix_r)
    loads[0].wait()
    start_plane(mix_copy)
    mix_w[core, tp] = mix_here[rows, pl.ds(pl.multiple_of(tp * T, T), T)]
    gain_copy = to_plane(lambda peer: norm_gain, gains.at[tp], gain_s, gain_r)
    start_plane(gain_copy)
    gains[tp] = norm_gain[...]
    product = values_in[...].astype(F32) * in_gate[...].astype(F32)
    docs = jnp.broadcast_to(documents[...], (8, T))
    tap = [column_of(conv_taps[j : j + 1, :], HEAD) for j in range(3)]
    gain_col = column_of(head_gain[...], HEAD)
    for halo in halos:
        halo.wait_recv()
    product_before = halo_v[...].astype(F32) * halo_g[...].astype(F32)
    docs_before = jnp.where(sp == 0, -1, jnp.broadcast_to(halo_d[...], (8, T)))
    convolved = jnp.zeros((HEAD, T), F32)
    for j in range(3):
        back = 2 - j
        if back:
            shifted = jnp.where(
                iota((HEAD, T), 1) < back,
                pltpu.roll(product_before, back, 1),
                pltpu.roll(product, back, 1),
            )
            docs_then = jnp.where(
                iota((8, T), 1) < back,
                pltpu.roll(docs_before, back, 1),
                pltpu.roll(docs, back, 1),
            )
            same = jnp.where(docs_then == docs, 1.0, 0.0)[0:1, :]
            convolved = convolved + tap[j] * shifted * same
        else:
            convolved = convolved + tap[j] * product
    mixed = out_gate[...].astype(F32) * convolved
    spread = jnp.mean(mixed * mixed, axis=0, keepdims=True)
    heads = (mixed * lax.rsqrt(spread + EPS) * gain_col).T.astype(BF16)

    head_all[tp] = heads
    head_copy = to_plane(lambda peer: head_all.at[tp], head_all.at[tp], head_s, head_r)
    start_plane(head_copy)

    downs = []
    for n, way in enumerate((1, -1, 2)):
        to_y, to_x = (y + way + SIDE) % SIDE, (x + way + SIDE) % SIDE
        downs.append(
            remote(w_down.at[to_y], w_one.at[y], down_s.at[2 * n], down_r.at[2 * n], tp=SIDE * to_y + x)
        )
        downs.append(
            remote(
                w_down.at[:, to_x],
                w_two.at[x],
                down_s.at[2 * n + 1],
                down_r.at[2 * n + 1],
                tp=SIDE * y + to_x,
            )
        )
    for load in loads[1:4]:
        load.wait()
    for copy in downs:
        copy.start()
    wait_plane(mix_copy)
    swap = remote(mix_w.at[core], mix_w.at[core], swap_s, swap_r, sp=2 * z + 1 - core)
    swap.start()
    total = stream[...].astype(F32).T
    swap.wait_recv()
    wait_plane(head_copy)
    half = HEAD // 2
    all_heads = jnp.concatenate([head_all[j] for j in range(N_TP)], axis=1)
    all_mix = jnp.concatenate(
        [mix_w[c, j] for j in range(N_TP) for c in range(2)], axis=0
    )
    total = total + dot(all_heads, all_mix)
    hidden[...] = total
    normed = (total * norm_gain[...]).astype(BF16)

    normed_all[y, x] = normed
    disp_out[...] = dot(pick[...], normed).astype(BF16).reshape(N_SP, CAP, T)
    order = [(dz, other) for dz in PLACES for other in (0, 1)][1:]

    def disp_copy(dz, other):
        place = PLACES.index(dz)
        expert = 2 * ((z - dz + N_Z) % N_Z) + ((core + 1 + other) % 2 if dz else 1 - core)
        block = 2 * place + core
        return remote(
            disp_out.at[expert],
            rows_all.at[y, x, block],
            disp_s.at[2 * place + other],
            disp_r.at[block],
            sp=expert,
        )

    def arrived(dz, other):
        place = PLACES.index(dz)
        return 2 * place + (other if dz else 1 - core)

    for dz, other in order:
        disp_copy(dz, other).start()
    own = core
    rows_all[y, x, own] = disp_out[sp]

    def wait_disp(chunk):
        for dz, other in order:
            if dz in DISTANCES[chunk]:
                block = arrived(dz, other)
                remote(
                    disp_out.at[0], rows_all.at[y, x, block], disp_s.at[0], disp_r.at[block], sp=behind
                ).wait_recv()

    def at_x(way):
        return (x + way + SIDE) % SIDE

    def at_y(way):
        return (y + way + SIDE) % SIDE

    to_x = [SIDE * y + at_x(-1), SIDE * y + at_x(1)]
    to_y = [SIDE * at_y(-1) + x, SIDE * at_y(1) + x]
    ways = (-1, 1)

    def numbered(moves, base):
        return [
            remote(src, dst, gat_s.at[base + n], gat_r.at[base + n], tp=peer)
            for n, (src, dst, peer) in enumerate(moves)
        ]

    def gather_copies(buf, start, size, base, stage, parity):
        both = pl.ds(start, size)
        one, two = pl.ds(start, size // 2), pl.ds(start + size // 2, size // 2)
        if stage == 0:
            moves = [(buf.at[y, x, both], to[i]) for i in (0, 1) for to in (to_x, to_y)]
        elif stage == 1:
            moves = [
                (buf.at[y, at_x(-1), one], to_x[1]),
                (buf.at[at_y(-1), x, two], to_y[1]),
                (buf.at[y, at_x(1), two], to_x[0]),
                (buf.at[at_y(1), x, one], to_y[0]),
            ]
            for i in (0, 1):
                for way in ways:
                    moves += [(buf.at[y, at_x(way), one], to_y[i]), (buf.at[at_y(way), x, two], to_x[i])]
        elif stage == 2:
            moves = []
            for i in (0, 1):
                moves += [(buf.at[y, at_x(2), one], to_y[i]), (buf.at[at_y(2), x, two], to_x[i])]
            moves += [
                (buf.at[at_y(-1), at_x(1), one], to_y[1]),
                (buf.at[at_y(1), at_x(-1), two], to_x[1]),
                (buf.at[at_y(1), at_x(-1), one], to_y[0]),
                (buf.at[at_y(-1), at_x(1), two], to_x[0]),
            ]
        else:
            i = parity
            moves = [
                (buf.at[at_y(-ways[i]), at_x(2), one], to_y[i]),
                (buf.at[at_y(2), at_x(-ways[i]), two], to_x[i]),
            ]
        return numbered([(ref, ref, peer) for ref, peer in moves], base + sum(GATHER[:stage]))

    def row_copies(chunk, stage):
        return gather_copies(rows_all, STARTS[chunk], SIZES[chunk], COPIES * chunk, stage, chunk % 2)

    def normed_copies(stage):
        return gather_copies(normed_all, 0, T, COPIES * CHUNKS, stage, 1)

    def halves(chunk):
        size = SIZES[chunk] // 4
        quarter = [pl.ds(STARTS[chunk] + n * size, size) for n in range(4)]
        return quarter[:2], quarter[2:]

    def expert_copies(chunk, stage):
        size = SIZES[chunk] // 2
        one, two = pl.ds(STARTS[chunk], size), pl.ds(STARTS[chunk] + size, size)
        (one_a, one_b), (two_a, two_b) = halves(chunk)
        moves = []
        if stage == 0:
            for i in (0, 1):
                moves += [(mid_all.at[y, x, one], to_x[i]), (mid_all.at[y, x, two], to_y[i])]
            moves = [(ref, ref, peer) for ref, peer in moves]
        elif stage == 1:
            moves = [
                (mid_all.at[y, at_x(-1), one_a], to_x[1]),
                (mid_all.at[at_y(-1), x, two_a], to_y[1]),
                (mid_all.at[y, at_x(1), one_b], to_x[0]),
                (mid_all.at[at_y(1), x, two_b], to_y[0]),
            ]
            moves = [(ref, ref, peer) for ref, peer in moves]
        elif stage == 2:
            for at, to, (a, b) in ((at_y, to_y, (one_a, one_b)), (at_x, to_x, (two_a, two_b))):
                moves += [(part.at[at(2), a], chain.at[a], to[1]), (part.at[at(2), b], chain.at[b], to[0])]
            for at, to, (a, b) in ((at_y, to_y, (one_a, one_b)), (at_x, to_x, (two_a, two_b))):
                moves += [(part.at[at(1), b], direct.at[b], to[1]), (part.at[at(-1), a], direct.at[a], to[0])]
        else:
            for to, (a, b) in ((to_y, (one_a, one_b)), (to_x, (two_a, two_b))):
                moves += [(chain_out.at[a], final.at[a], to[1]), (chain_out.at[b], final.at[b], to[0])]
        return numbered(moves, COPIES * chunk + sum(GATHER) + sum(EXPERT[:stage]))

    def go(copies):
        for copy in copies:
            copy.start()

    def got(copies):
        for copy in copies:
            copy.wait_recv()

    def rows_of(ref):
        return ref.reshape(ref.shape[0] * CAP, T)

    def silu(v):
        return v / (1.0 + jnp.exp(-v))

    def gated(blocks, weights):
        squares = jnp.zeros(blocks[0].shape, F32)
        for j, block in enumerate(blocks):
            wide = block.astype(F32)
            squares = squares + wide * wide * (1.0 / (gains[j] * gains[j]))
        scale = lax.rsqrt(jnp.sum(squares, axis=1, keepdims=True) / D + EPS)
        pair = dot(jnp.concatenate(blocks, axis=1), weights) * scale
        return (silu(pair[:, :T]) * pair[:, T:]).astype(BF16)

    def gate_up(chunk):
        here = pl.ds(STARTS[chunk], SIZES[chunk])
        blocks = [rows_of(rows_all[i, j, here]) for i in range(SIDE) for j in range(SIDE)]
        mid = gated(blocks, w_gu[...])
        mid_all[y, x, here] = mid.reshape(SIZES[chunk], CAP, T)

    def down(chunk):
        size = SIZES[chunk] // 2
        for half in range(2):
            here = pl.ds(STARTS[chunk] + size * half, size)
            line = [mid_all[y, k, here] if half == 0 else mid_all[k, x, here] for k in range(SIDE)]
            line = jnp.concatenate([rows_of(block) for block in line], axis=1)
            weights = w_two if half else w_one
            for q in range(0, SIDE, 2):
                pair = jnp.concatenate(
                    [weights[q + n].reshape(SIDE * T, T) for n in range(2)], axis=1
                )
                result = dot(line, pair).astype(BF16)
                for n in range(2):
                    part[q + n, here] = result[:, n * T : (n + 1) * T].reshape(size, CAP, T)

    def relay(chunk):
        for at, (a, b) in zip((at_y, at_x), halves(chunk)):
            for rows, q in ((a, at(1)), (b, at(-1))):
                chain_out[rows] = (chain[rows].astype(F32) + part[q, rows].astype(F32)).astype(BF16)

    def finish(chunk):
        for own_place, (a, b) in zip((y, x), halves(chunk)):
            for rows in (a, b):
                value = part[own_place, rows].astype(F32) + direct[rows].astype(F32)
                ret_out[rows] = (value + final[rows].astype(F32)).astype(BF16)

    def ret_copy(dz, other):
        place = PLACES.index(dz)
        group_core = (core + 1 + other) % 2 if dz else 1 - core
        group = 2 * ((z + dz + N_Z) % N_Z) + group_core
        return remote(
            ret_out.at[2 * place + group_core],
            ret_in.at[sp],
            ret_s.at[2 * place + other],
            ret_r.at[2 * place + core],
            sp=group,
        )

    def start_ret(chunk):
        for dz, other in order:
            if dz in DISTANCES[chunk]:
                ret_copy(dz, other).start()

    def shared_expert():
        for load in loads[4:7]:
            load.wait()
        mid = gated([normed_all[i, j] for i in range(SIDE) for j in range(SIDE)], s_gu[...])
        for j in range(N_TP // 2):
            part = dot(mid, s_down[:, 2 * T * j : 2 * T * (j + 1)]).astype(BF16)
            sh_part[2 * j] = part[:, :T]
            sh_part[2 * j + 1] = part[:, T:]

    sh_copy = to_plane(lambda peer: sh_part.at[peer], sh_in.at[tp], sh_s, sh_r)

    def advance(chunk, stage):
        if stage == 0:
            wait_disp(chunk)
            go(row_copies(chunk, 0))
        elif stage < 4:
            got(row_copies(chunk, stage - 1))
            go(row_copies(chunk, stage))
        elif stage == 4:
            got(row_copies(chunk, 3))
            gate_up(chunk)
            go(expert_copies(chunk, 0))
        elif stage == 5:
            got(expert_copies(chunk, 0))
            go(expert_copies(chunk, 1))
        elif stage == 6:
            got(expert_copies(chunk, 1))
            down(chunk)
            go(expert_copies(chunk, 2))
        elif stage == 7:
            got(expert_copies(chunk, 2))
            relay(chunk)
            go(expert_copies(chunk, 3))
        else:
            got(expert_copies(chunk, 3))
            finish(chunk)
            start_ret(chunk)

    go(normed_copies(0))
    steps = sorted((stage + LAG * chunk, chunk, stage) for chunk in range(CHUNKS) for stage in range(STAGES))
    for _, chunk, stage in steps:
        if (chunk, stage) == (0, 4):
            wait_plane(gain_copy)
            for load in loads[7:]:
                load.wait()
            got(downs)
        advance(chunk, stage)
        for turn, after in SHARED.items():
            if after == (chunk, stage):
                got(normed_copies(turn - 1))
                if turn < 4:
                    go(normed_copies(turn))
                else:
                    shared_expert()
                    sh_in[tp] = sh_part[tp]
        if (chunk, stage) == SHARED_SEND_AFTER:
            start_plane(sh_copy)
        if (chunk, stage) == (0, 8):
            ret_in[sp] = ret_out[own]

    wait_plane(sh_copy)
    total = hidden[...]
    for j in range(N_TP):
        total = total + sh_in[j].astype(F32)

    for halo in halos:
        halo.wait_send()
    swap.wait_send()
    for copy in (mix_copy, gain_copy, head_copy, sh_copy):

        @pl.loop(1, N_TP)
        def _(step, copy=copy):
            copy(step).wait_send()

    for dz, other in order:
        disp_copy(dz, other).wait_send()
    sent = downs[:]
    for stage in range(4):
        sent += normed_copies(stage)
        for chunk in range(CHUNKS):
            sent += row_copies(chunk, stage) + expert_copies(chunk, stage)
    for copy in sent:
        copy.wait_send()

    for dz, other in order:
        block = arrived(dz, other)
        remote(ret_out.at[0], ret_in.at[0], ret_s.at[0], ret_r.at[block], sp=behind).wait_recv()
    returned = ret_in[...].reshape(SLOTS, T)
    total = total + dot(comb_hi[...], returned) + dot(comb_lo[...], returned)
    out[...] = total.T.astype(BF16)
    for dz, other in order:
        ret_copy(dz, other).wait_send()


def local(
    stream,
    values_in,
    in_gate,
    out_gate,
    documents,
    conv_taps,
    head_gain,
    mix_weight,
    norm_gain,
    routes,
    route_weight,
    expert_gate,
    expert_up,
    expert_down,
    shared_gate,
    shared_up,
    shared_down,
):
    vmem = pl.BlockSpec(memory_space=pltpu.VMEM)
    hbm = pl.BlockSpec(memory_space=pl.ANY)
    dma = pltpu.SemaphoreType.DMA
    return pl.pallas_call(
        kernel,
        name="layer",
        out_shape=jax.ShapeDtypeStruct((T, T), BF16),
        in_specs=[vmem] * 7 + [hbm] + [vmem] * 3 + [hbm] * 6,
        out_specs=vmem,
        scratch_shapes=[
            pltpu.VMEM((HEAD, T), BF16),
            pltpu.VMEM((HEAD, T), BF16),
            pltpu.VMEM((1, T), jnp.int32),
            pltpu.VMEM((HEAD, D), BF16),
            pltpu.VMEM((2, N_TP, HEAD // 2, T), BF16),
            pltpu.VMEM((D, 2 * T), BF16),
            pltpu.VMEM((SIDE, SIDE, T, T), BF16),
            pltpu.VMEM((SIDE, SIDE, T, T), BF16),
            pltpu.VMEM((SIDE, SIDE, T, T), BF16),
            pltpu.VMEM((D, 2 * T), BF16),
            pltpu.VMEM((T, D), BF16),
            pltpu.VMEM((N_TP, T, HEAD), BF16),
            pltpu.VMEM((N_TP, 1, T), F32),
            pltpu.VMEM((SIDE, SIDE, T, T), BF16),
            pltpu.VMEM((SLOTS, T), BF16),
            pltpu.VMEM((T, SLOTS), BF16),
            pltpu.VMEM((T, SLOTS), BF16),
            pltpu.VMEM((N_SP, CAP, T), BF16),
            pltpu.VMEM((SIDE, SIDE, N_SP, CAP, T), BF16),
            pltpu.VMEM((SIDE, SIDE, N_SP, CAP, T), BF16),
            pltpu.VMEM((SIDE, N_SP, CAP, T), BF16),
            pltpu.VMEM((N_SP, CAP, T), BF16),
            pltpu.VMEM((N_SP, CAP, T), BF16),
            pltpu.VMEM((N_SP, CAP, T), BF16),
            pltpu.VMEM((N_SP, CAP, T), BF16),
            pltpu.VMEM((N_SP, CAP, T), BF16),
            pltpu.VMEM((N_SP, CAP, T), BF16),
            pltpu.VMEM((N_TP, T, T), BF16),
            pltpu.VMEM((N_TP, T, T), BF16),
            pltpu.VMEM((T, T), F32),
            dma((9,)),
            dma((6,)),
            dma((6,)),
            dma((3,)),
            dma((3,)),
            dma((N_TP,)),
            dma((N_TP,)),
            dma,
            dma,
            dma((N_TP,)),
            dma((N_TP,)),
            dma((N_TP,)),
            dma((N_TP,)),
            dma((N_TP,)),
            dma((N_TP,)),
            dma((N_SP,)),
            dma((N_SP,)),
            dma((ALL,)),
            dma((ALL,)),
            dma((N_SP,)),
            dma((N_SP,)),
            dma((N_TP,)),
            dma((N_TP,)),
        ],
        compiler_params=pltpu.CompilerParams(collective_id=0, has_side_effects=True),
    )(
        stream,
        values_in,
        in_gate,
        out_gate,
        documents[None, :],
        conv_taps,
        head_gain[None, :],
        mix_weight,
        norm_gain[None, :],
        routes.T,
        route_weight.T,
        expert_gate,
        expert_up,
        expert_down.reshape(SIDE, SIDE, T, T),
        shared_gate,
        shared_up,
        shared_down,
    )


def solution(mesh):
    in_specs = (
        P("tp", "sp"),
        P("tp", "sp"),
        P("tp", "sp"),
        P("tp", "sp"),
        P("sp"),
        P(None, "tp"),
        P("tp"),
        P("tp", None),
        P("tp"),
        P("sp", None),
        P("sp", None),
        P("sp", None, "tp"),
        P("sp", None, "tp"),
        P("sp", None, "tp"),
        P(None, "tp"),
        P(None, "tp"),
        P("tp", None),
    )
    return jax.shard_map(
        local, mesh=mesh, in_specs=in_specs, out_specs=P("tp", "sp"), check_vma=False
    )
```

time: 109 us -> 94.2 us (0.86)
  Pallas kernels: 105 us -> 92.6 us
  local copies, waits for them, and re-layouts: 3.51 us -> 1.38 us
    pallas_call x1, Pallas kernels: 105 us -> 92.6 us  [local(): pl.pallas_call(kernel, name='layer', out_shape=jax.ShapeDtypeStruct((T, T...]
    unnamed x7 -> x1, local copies, waits for them, and re-layouts: 3.51 us -> 1.38 us
where the time goes in v2:
time: 94.2 us; the launch traced here: 93.9 us
  Pallas kernels  92.6 us (98%)
  local copies, waits for them, and re-layouts  1.38 us (1%)
    pallas_call x1, Pallas kernels, local(): pl.pallas_call(kernel, name='layer', out_shape=jax.ShapeDtypeStruct((T, T...  92.6 us

profile of v2, /device:TPU:1, one launch (start us, length us, event | category | flops | bytes accessed | tf_op | source)
XLA Modules:
  0.0 93.9 jit_solution(7572888945902999507)
XLA Ops:
  0.0 92.6 %layer.1 = bf16[128,128]{1,0:T(8,128)(2,1)} custom-call(bf16[128,128]{1,0:T(8,128)(2,1)} %stream.1, bf16[64,128]{1,0:T(8,128)(2,1)} %values_in.1, bf16[64,128]{1,0:T(8,128)(2,1)} %in_gate.1, bf16[64,128]{1,0:T(8,128)(2,1)} %out_gate.1, s32[1,128]{1,0:T(1,128)} %bitcast.9, f32[3,64]{1,0:T(4,128)} %conv_taps.1, f32[1,64]{1,0:T(1,128)} %bitcast.10, ...), custom_call_target="tpu_custom_call" | custom-call | tf_op jit(solution)/shard_map/layer/pallas_call | solution.py:621
  92.6 1.4 %copy.19 = bf16[128,128]{1,0:T(8,128)(2,1)} copy(bf16[128,128]{1,0:T(8,128)(2,1)} %layer.1) | data formatting | bytes 65536

commit v3 on v2

v3 whole, which is shorter than its diff:
```python
import jax
import jax.numpy as jnp
from jax import lax
from jax.experimental import pallas as pl
from jax.experimental.pallas import tpu as pltpu
from jax.sharding import PartitionSpec as P

F32 = jnp.float32
BF16 = jnp.bfloat16
MESH = pl.DeviceIdType.MESH
EPS = 1e-06

D = 2048
T = 128
HEAD = 64
N_SP = 32
N_TP = 16
N_Z = 16
SIDE = 4
CAP = 24
TOP_K = 4
SLOTS = N_SP * CAP
DISTANCES = ((0, 1, -1, 2), (8, -7, 7, -6, 6, -5, 5, -4), (4, -3, 3, -2))
PLACES = [dz for chunk in DISTANCES for dz in chunk]
CHUNKS = len(DISTANCES)
SIZES = [2 * len(chunk) for chunk in DISTANCES]
STARTS = [sum(SIZES[:c]) for c in range(CHUNKS)]
DIRECT = (True, False, True)
STEPS = 5
LAG = 1.01
SHARED = ((1, 0), (1, 1), (1, 3))
SHARED_SEND_AFTER = (CHUNKS - 1, -2)


def dot(a, b, contract=((1,), (0,)), precision=None):
    return lax.dot_general(
        a, b, (contract, ((), ())), precision=precision, preferred_element_type=F32
    )


def iota(shape, dim):
    return lax.broadcasted_iota(jnp.int32, shape, dim)


def column_of(row, n):
    eye = iota((n, n), 0) == iota((n, n), 1)
    return jnp.sum(jnp.where(eye, jnp.broadcast_to(row, (n, n)), 0.0), axis=1, keepdims=True)


def kernel(
    stream,
    values_in,
    in_gate,
    out_gate,
    documents,
    conv_taps,
    head_gain,
    mix_weight,
    norm_gain,
    routes,
    route_weight,
    expert_gate,
    expert_up,
    expert_down,
    shared_gate,
    shared_up,
    shared_down,
    out,
    halo_v,
    halo_g,
    halo_d,
    mix_here,
    mix_w,
    w_gu,
    w_down,
    w_one,
    w_two,
    s_gu,
    s_down,
    head_all,
    gains,
    normed_all,
    pick,
    comb_hi,
    comb_lo,
    disp_out,
    rows_all,
    mid_all,
    part,
    direct,
    ret_out,
    ret_in,
    sh_part,
    sh_in,
    hidden,
    load_sem,
    down_s,
    down_r,
    halo_s,
    halo_r,
    mix_s,
    mix_r,
    swap_s,
    swap_r,
    head_s,
    head_r,
    tail_s,
    tail_r,
    gain_s,
    gain_r,
    disp_s,
    disp_r,
    gat_s,
    gat_r,
    ret_s,
    ret_r,
    sh_s,
    sh_r,
):
    sp = lax.axis_index("sp")
    tp = lax.axis_index("tp")
    z, core = sp // 2, sp % 2
    y, x = tp // SIDE, tp % SIDE

    def remote(src, dst, send, recv, **where):
        return pltpu.make_async_remote_copy(
            src_ref=src,
            dst_ref=dst,
            send_sem=send,
            recv_sem=recv,
            device_id=where,
            device_id_type=MESH,
        )

    barrier = pltpu.get_barrier_semaphore()

    @pl.loop(1, N_SP)
    def _(step):
        pl.semaphore_signal(
            barrier, inc=1, device_id={"sp": (sp + step) % N_SP}, device_id_type=MESH
        )

    @pl.loop(1, N_TP)
    def _(step):
        pl.semaphore_signal(
            barrier, inc=1, device_id={"tp": (tp + step) % N_TP}, device_id_type=MESH
        )

    loads = [
        pltpu.make_async_copy(src, dst, load_sem.at[i])
        for i, (src, dst) in enumerate(
            [
                (mix_weight, mix_here),
                (expert_down, w_down),
                (expert_down.at[y], w_one.at[y]),
                (expert_down.at[:, x], w_two.at[x]),
                (shared_gate, s_gu.at[:, pl.ds(0, T)]),
                (shared_up, s_gu.at[:, pl.ds(T, T)]),
                (shared_down, s_down),
                (expert_gate.at[0], w_gu.at[:, pl.ds(0, T)]),
                (expert_up.at[0], w_gu.at[:, pl.ds(T, T)]),
            ]
        )
    ]
    for load in loads:
        load.start()

    line = iota((T, T), 0)
    named = jnp.zeros((T, T), F32)
    weight = jnp.zeros((T, T), F32)
    for k in range(TOP_K):
        hit = routes[k : k + 1, :] == line
        named = jnp.where(hit, 1.0, named)
        weight = jnp.where(hit, route_weight[k : k + 1, :], weight)
    before = jnp.where(line < iota((T, T), 1), 1.0, 0.0).astype(BF16)
    earlier = dot(named.astype(BF16), before)
    slot = jnp.where(named > 0, earlier, 200.0)
    slot_t = slot.T.astype(BF16)
    slot = slot.astype(BF16)
    weight = weight.T

    def slot_number(shape, dim):
        number = iota(shape, dim).astype(F32)
        return number - CAP * jnp.floor((number + 0.5) * (1.0 / CAP))

    away = iota((SLOTS, T), 0) - CAP * iota((SLOTS, T), 1)
    owner = jnp.where((away >= 0) & (away < CAP), 1.0, 0.0).astype(BF16)
    taken = dot(owner, slot)
    pick[...] = jnp.where(taken == slot_number((SLOTS, T), 0), 1.0, 0.0).astype(BF16)
    away = iota((T, SLOTS), 1) - CAP * iota((T, SLOTS), 0)
    owner = jnp.where((away >= 0) & (away < CAP), 1.0, 0.0).astype(BF16)
    taken = dot(slot_t, owner) == slot_number((T, SLOTS), 1)
    weight_hi = weight.astype(BF16)
    weight_lo = (weight - weight_hi.astype(F32)).astype(BF16)
    comb_hi[...] = jnp.where(taken, dot(weight_hi, owner), 0.0).astype(BF16)
    comb_lo[...] = jnp.where(taken, dot(weight_lo, owner), 0.0).astype(BF16)

    pl.semaphore_wait(barrier, N_SP + N_TP - 2)

    behind = (sp + 1) % N_SP
    halos = [
        remote(src, dst, halo_s.at[i], halo_r.at[i], sp=behind)
        for i, (src, dst) in enumerate(
            [(values_in, halo_v), (in_gate, halo_g), (documents, halo_d)]
        )
    ]
    for halo in halos:
        halo.start()

    def arrive(ref, recv):
        remote(ref, ref, recv, recv, sp=behind).wait_recv()

    def leave(ref, send):
        remote(ref, ref, send, send, sp=behind).wait_send()

    def to_plane(src_of, dst, send, recv):
        @pl.loop(1, N_TP)
        def _(step):
            peer = (tp + step) % N_TP
            remote(src_of(peer), dst, send, recv, tp=peer).start()

    rows = pl.ds(pl.multiple_of(core * (HEAD // 2), HEAD // 2), HEAD // 2)

    def columns(peer):
        return mix_here.at[rows, pl.ds(pl.multiple_of(peer * T, T), T)]

    loads[0].wait()
    to_plane(columns, mix_w.at[tp, rows], mix_s, mix_r)
    mix_w[tp, rows] = mix_here[rows, pl.ds(pl.multiple_of(tp * T, T), T)]

    product = values_in[...].astype(F32) * in_gate[...].astype(F32)
    docs = jnp.broadcast_to(documents[...], (8, T))
    tap = [column_of(conv_taps[j : j + 1, :], HEAD) for j in range(3)]
    gain_col = column_of(head_gain[...], HEAD)

    def heads_after(product_before, docs_before):
        convolved = jnp.zeros((HEAD, T), F32)
        for j in range(3):
            back = 2 - j
            if back:
                shifted = jnp.where(
                    iota((HEAD, T), 1) < back,
                    pltpu.roll(product_before, back, 1),
                    pltpu.roll(product, back, 1),
                )
                docs_then = jnp.where(
                    iota((8, T), 1) < back,
                    pltpu.roll(docs_before, back, 1),
                    pltpu.roll(docs, back, 1),
                )
                same = jnp.where(docs_then == docs, 1.0, 0.0)[0:1, :]
                convolved = convolved + tap[j] * shifted * same
            else:
                convolved = convolved + tap[j] * product
        mixed = out_gate[...].astype(F32) * convolved
        spread = jnp.mean(mixed * mixed, axis=0, keepdims=True)
        heads = (mixed * lax.rsqrt(spread + EPS) * gain_col).T
        return jnp.concatenate([heads[:HEAD], heads[HEAD:]], axis=1).astype(BF16)

    first, rest = pl.ds(0, 8), pl.ds(8, HEAD - 8)
    head_all[tp, rest] = heads_after(product, docs)[8:]
    to_plane(lambda peer: head_all.at[tp, rest], head_all.at[tp, rest], head_s, head_r)
    for halo in halos:
        halo.wait_recv()
    product_before = halo_v[...].astype(F32) * halo_g[...].astype(F32)
    docs_before = jnp.where(sp == 0, -1, jnp.broadcast_to(halo_d[...], (8, T)))
    head_all[tp, first] = heads_after(product_before, docs_before)[:8]
    to_plane(lambda peer: head_all.at[tp, first], head_all.at[tp, first], tail_s, tail_r)

    others = pl.ds(0, N_TP - 1)
    arrive(mix_w.at[others, pl.ds(0, HEAD // 2)], mix_r)
    swap = remote(mix_w.at[:, rows], mix_w.at[:, rows], swap_s, swap_r, sp=2 * z + 1 - core)
    swap.start()
    for load in loads[1:4]:
        load.wait()
    for way in (2, -1, 1):
        beside_y, beside_x = (y + way + SIDE) % SIDE, (x + way + SIDE) % SIDE
        remote(
            w_down.at[beside_y], w_one.at[y], down_s.at[0], down_r.at[0], tp=SIDE * beside_y + x
        ).start()
        remote(
            w_down.at[:, beside_x], w_two.at[x], down_s.at[1], down_r.at[1], tp=SIDE * y + beside_x
        ).start()

    total = stream[...].astype(F32).T
    swap.wait_recv()
    arrive(head_all.at[others, rest], head_r)
    arrive(head_all.at[others, first], tail_r)
    all_heads = jnp.concatenate([head_all[j] for j in range(N_TP)], axis=1)
    none = jnp.zeros((HEAD, T), BF16)
    early = jnp.concatenate([v for j in range(N_TP) for v in (mix_w[j], none)], axis=0)
    late = jnp.concatenate([v for j in range(N_TP) for v in (none, mix_w[j])], axis=0)
    mixer = dot(all_heads, jnp.concatenate([early, late], axis=1))
    total = total + jnp.concatenate([mixer[:, :T], mixer[:, T:]], axis=0)
    hidden[...] = total
    normed = (total * norm_gain[...]).astype(BF16)

    normed_all[y, x] = normed
    disp_out[...] = dot(pick[...], normed).astype(BF16).reshape(N_SP, CAP, T)
    order = [(dz, other) for dz in PLACES for other in (0, 1)][1:]

    def disp_copy(dz, other):
        place = PLACES.index(dz)
        expert = 2 * ((z - dz + N_Z) % N_Z) + ((core + 1 + other) % 2 if dz else 1 - core)
        block = 2 * place + core
        return remote(
            disp_out.at[expert],
            rows_all.at[y, x, block],
            disp_s,
            disp_r.at[next(c for c in range(CHUNKS) if dz in DISTANCES[c])],
            sp=expert,
        )

    for dz, other in order:
        disp_copy(dz, other).start()
    own = core
    rows_all[y, x, own] = disp_out[sp]

    def wait_disp(chunk):
        count = SIZES[chunk] - (chunk == 0)
        arrive(rows_all.at[y, x, pl.ds(STARTS[chunk], count)], disp_r.at[chunk])

    def at_x(way):
        return (x + way + SIDE) % SIDE

    def at_y(way):
        return (y + way + SIDE) % SIDE

    to_x = [SIDE * y + at_x(-1), SIDE * y + at_x(1)]
    to_y = [SIDE * at_y(-1) + x, SIDE * at_y(1) + x]
    ways = (-1, 1)

    def numbered(moves, index):
        return [
            remote(src, dst, gat_s.at[index], gat_r.at[index], tp=peer) for src, dst, peer in moves
        ]

    to_x.append(SIDE * y + at_x(2))
    to_y.append(SIDE * at_y(2) + x)

    def gather_copies(buf, start, size, index, stage, short):
        both = pl.ds(start, size)
        one, two = pl.ds(start, size // 2), pl.ds(start + size // 2, size // 2)
        a, b = pl.ds(start, size // 4), pl.ds(start + size // 4, size // 4)
        c, d = pl.ds(start + size // 2, size // 4), pl.ds(start + size // 2 + size // 4, size // 4)
        if stage == 0:
            moves = [(buf.at[y, x, both], to[i]) for i in (2, 0, 1) for to in (to_x, to_y)]
        elif stage == 1:
            moves = []
            for way in (-1, 1, 2):
                for i in (2, 0, 1) if short else (0, 1):
                    moves += [(buf.at[y, at_x(way), one], to_y[i]), (buf.at[at_y(way), x, two], to_x[i])]
        else:
            moves = [
                (buf.at[at_y(-1), at_x(1), one], to_y[1]),
                (buf.at[at_y(1), at_x(-1), two], to_x[1]),
                (buf.at[at_y(1), at_x(-1), one], to_y[0]),
                (buf.at[at_y(-1), at_x(1), two], to_x[0]),
                (buf.at[at_y(-1), at_x(2), a], to_y[1]),
                (buf.at[at_y(2), at_x(-1), c], to_x[1]),
                (buf.at[at_y(1), at_x(2), b], to_y[0]),
                (buf.at[at_y(2), at_x(1), d], to_x[0]),
            ]
        return numbered([(ref, ref, peer) for ref, peer in moves], index)

    def thirds(stage, short):
        return (2, 3 if short else 2, 1)[stage]

    def row_copies(chunk, stage):
        index = STEPS * chunk + stage
        start, size, short = STARTS[chunk], SIZES[chunk], DIRECT[chunk]
        copies = lambda: gather_copies(rows_all, start, size, index, stage, short)
        count = thirds(stage, DIRECT[chunk])
        return copies, rows_all.at[pl.ds(0, count), pl.ds(0, 3), pl.ds(0, SIZES[chunk])], index

    def normed_copies(stage):
        index = STEPS * CHUNKS + stage
        copies = lambda: gather_copies(normed_all, 0, T, index, stage, False)
        return copies, normed_all.at[pl.ds(0, thirds(stage, False)), pl.ds(0, 3)], index

    def expert_copies(chunk, stage):
        size = SIZES[chunk] // 2
        one, two = pl.ds(STARTS[chunk], size), pl.ds(STARTS[chunk] + size, size)
        moves = []
        for i, way in ((2, 2), (0, -1), (1, 1)):
            if stage == 0:
                moves.append((mid_all.at[y, x, one], mid_all.at[y, x, one], to_x[i]))
                moves.append((mid_all.at[y, x, two], mid_all.at[y, x, two], to_y[i]))
            else:
                moves.append((part.at[at_y(way), one], direct.at[i, one], to_y[i]))
                moves.append((part.at[at_x(way), two], direct.at[i, two], to_x[i]))
        index = STEPS * chunk + 3 + stage
        return lambda: numbered(moves, index), direct.at[:, pl.ds(0, SIZES[chunk])], index

    def go(kind):
        for copy in kind[0]():
            copy.start()

    def got(kind):
        arrive(kind[1], gat_r.at[kind[2]])

    def rows_of(ref):
        return ref.reshape(ref.shape[0] * CAP, T)

    def silu(v):
        return v / (1.0 + jnp.exp(-v))

    def gated(blocks, weights):
        squares = jnp.zeros(blocks[0].shape, F32)
        for j, block in enumerate(blocks):
            wide = block.astype(F32)
            squares = squares + wide * wide * (1.0 / (gains[j] * gains[j]))
        scale = lax.rsqrt(jnp.sum(squares, axis=1, keepdims=True) / D + EPS)
        pair = dot(jnp.concatenate(blocks, axis=1), weights) * scale
        return (silu(pair[:, :T]) * pair[:, T:]).astype(BF16)

    def gate_up(chunk):
        here = pl.ds(STARTS[chunk], SIZES[chunk])
        blocks = [rows_of(rows_all[i, j, here]) for i in range(SIDE) for j in range(SIDE)]
        mid = gated(blocks, w_gu[...])
        mid_all[y, x, here] = mid.reshape(SIZES[chunk], CAP, T)

    def down(chunk):
        size = SIZES[chunk] // 2
        for half in range(2):
            here = pl.ds(STARTS[chunk] + size * half, size)
            line = [mid_all[y, k, here] if half == 0 else mid_all[k, x, here] for k in range(SIDE)]
            line = jnp.concatenate([rows_of(block) for block in line], axis=1)
            weights = w_two if half else w_one
            for q in range(0, SIDE, 2):
                pair = jnp.concatenate(
                    [weights[q + n].reshape(SIDE * T, T) for n in range(2)], axis=1
                )
                result = dot(line, pair).astype(BF16)
                for n in range(2):
                    part[q + n, here] = result[:, n * T : (n + 1) * T].reshape(size, CAP, T)

    def finish(chunk):
        size = SIZES[chunk] // 2
        for half in range(2):
            here = pl.ds(STARTS[chunk] + size * half, size)
            value = part[x if half else y, here].astype(F32)
            for i in range(3):
                value = value + direct[i, here].astype(F32)
            ret_out[here] = value.astype(BF16)

    def ret_copy(dz, other):
        place = PLACES.index(dz)
        group_core = (core + 1 + other) % 2 if dz else 1 - core
        group = 2 * ((z + dz + N_Z) % N_Z) + group_core
        return remote(
            ret_out.at[2 * place + group_core],
            ret_in.at[sp],
            ret_s,
            ret_r,
            sp=group,
        )

    def start_ret(chunk):
        for dz, other in order:
            if dz in DISTANCES[chunk]:
                ret_copy(dz, other).start()

    def shared_expert():
        for load in loads[4:7]:
            load.wait()
        mid = gated([normed_all[i, j] for i in range(SIDE) for j in range(SIDE)], s_gu[...])
        for j in range(N_TP // 2):
            part = dot(mid, s_down[:, 2 * T * j : 2 * T * (j + 1)]).astype(BF16)
            sh_part[2 * j] = part[:, :T]
            sh_part[2 * j + 1] = part[:, T:]

    def row_stages(chunk):
        return 2 if DIRECT[chunk] else 3

    def advance(chunk, stage):
        rows = row_stages(chunk)
        if stage == 0:
            wait_disp(chunk)
            go(row_copies(chunk, 0))
        elif stage < rows:
            got(row_copies(chunk, stage - 1))
            go(row_copies(chunk, stage))
        elif stage == rows:
            got(row_copies(chunk, rows - 1))
            gate_up(chunk)
            go(expert_copies(chunk, 0))
        elif stage == rows + 1:
            got(expert_copies(chunk, 0))
            down(chunk)
            go(expert_copies(chunk, 1))
        else:
            got(expert_copies(chunk, 1))
            finish(chunk)
            start_ret(chunk)

    go(normed_copies(0))
    to_plane(lambda peer: norm_gain, gains.at[tp], gain_s, gain_r)
    gains[tp] = norm_gain[...]
    steps = sorted(
        (stage + LAG * chunk, chunk, stage)
        for chunk in range(CHUNKS)
        for stage in range(row_stages(chunk) + 3)
    )
    for _, chunk, stage in steps:
        left = stage - row_stages(chunk) - 3
        if (chunk, left) == (0, -3):
            arrive(gains.at[others], gain_r)
            for load in loads[7:]:
                load.wait()
        if (chunk, left) == (0, -2):
            arrive(w_one.at[pl.ds(0, 3)], down_r.at[0])
            arrive(w_two.at[pl.ds(0, 3)], down_r.at[1])
        advance(chunk, stage)
        for turn, after in enumerate(SHARED):
            if after == (chunk, stage):
                got(normed_copies(turn))
                if turn < 2:
                    go(normed_copies(turn + 1))
                else:
                    shared_expert()
                    sh_in[tp] = sh_part[tp]
        if (chunk, left) == SHARED_SEND_AFTER:
            to_plane(lambda peer: sh_part.at[peer], sh_in.at[tp], sh_s, sh_r)
        if (chunk, left) == (0, -1):
            ret_in[sp] = ret_out[own]

    arrive(sh_in.at[others], sh_r)
    total = hidden[...]
    for j in range(N_TP):
        total = total + sh_in[j].astype(F32)

    for halo in halos:
        halo.wait_send()
    swap.wait_send()
    for ref, send in (
        (mix_w.at[others, pl.ds(0, HEAD // 2)], mix_s),
        (head_all.at[others, rest], head_s),
        (head_all.at[others, first], tail_s),
        (gains.at[others], gain_s),
        (w_one.at[pl.ds(0, 3)], down_s.at[0]),
        (w_two.at[pl.ds(0, 3)], down_s.at[1]),
        (disp_out.at[pl.ds(0, N_SP - 1)], disp_s),
        (sh_in.at[others], sh_s),
    ):
        leave(ref, send)
    kinds = [normed_copies(stage) for stage in range(3)]
    for chunk in range(CHUNKS):
        kinds += [row_copies(chunk, stage) for stage in range(row_stages(chunk))]
        kinds += [expert_copies(chunk, stage) for stage in range(2)]
    for _, ref, index in kinds:
        leave(ref, gat_s.at[index])

    arrive(ret_in.at[pl.ds(0, N_SP - 1)], ret_r)
    returned = ret_in[...].reshape(SLOTS, T)
    total = total + dot(comb_hi[...], returned) + dot(comb_lo[...], returned)
    out[...] = total.T.astype(BF16)
    leave(ret_in.at[pl.ds(0, N_SP - 1)], ret_s)


def local(
    stream,
    values_in,
    in_gate,
    out_gate,
    documents,
    conv_taps,
    head_gain,
    mix_weight,
    norm_gain,
    routes,
    route_weight,
    expert_gate,
    expert_up,
    expert_down,
    shared_gate,
    shared_up,
    shared_down,
):
    vmem = pl.BlockSpec(memory_space=pltpu.VMEM)
    hbm = pl.BlockSpec(memory_space=pl.ANY)
    dma = pltpu.SemaphoreType.DMA
    return pl.pallas_call(
        kernel,
        name="layer",
        out_shape=jax.ShapeDtypeStruct((T, T), BF16),
        in_specs=[vmem] * 7 + [hbm] + [vmem] * 3 + [hbm] * 6,
        out_specs=vmem,
        scratch_shapes=[
            pltpu.VMEM((HEAD, T), BF16),
            pltpu.VMEM((HEAD, T), BF16),
            pltpu.VMEM((1, T), jnp.int32),
            pltpu.VMEM((HEAD, D), BF16),
            pltpu.VMEM((N_TP, HEAD, T), BF16),
            pltpu.VMEM((D, 2 * T), BF16),
            pltpu.VMEM((SIDE, SIDE, T, T), BF16),
            pltpu.VMEM((SIDE, SIDE, T, T), BF16),
            pltpu.VMEM((SIDE, SIDE, T, T), BF16),
            pltpu.VMEM((D, 2 * T), BF16),
            pltpu.VMEM((T, D), BF16),
            pltpu.VMEM((N_TP, HEAD, T), BF16),
            pltpu.VMEM((N_TP, 1, T), F32),
            pltpu.VMEM((SIDE, SIDE, T, T), BF16),
            pltpu.VMEM((SLOTS, T), BF16),
            pltpu.VMEM((T, SLOTS), BF16),
            pltpu.VMEM((T, SLOTS), BF16),
            pltpu.VMEM((N_SP, CAP, T), BF16),
            pltpu.VMEM((SIDE, SIDE, N_SP, CAP, T), BF16),
            pltpu.VMEM((SIDE, SIDE, N_SP, CAP, T), BF16),
            pltpu.VMEM((SIDE, N_SP, CAP, T), BF16),
            pltpu.VMEM((3, N_SP, CAP, T), BF16),
            pltpu.VMEM((N_SP, CAP, T), BF16),
            pltpu.VMEM((N_SP, CAP, T), BF16),
            pltpu.VMEM((N_TP, T, T), BF16),
            pltpu.VMEM((N_TP, T, T), BF16),
            pltpu.VMEM((T, T), F32),
            dma((9,)),
            dma((2,)),
            dma((2,)),
            dma((3,)),
            dma((3,)),
            dma,
            dma,
            dma,
            dma,
            dma,
            dma,
            dma,
            dma,
            dma,
            dma,
            dma,
            dma((CHUNKS,)),
            dma((STEPS * CHUNKS + 3,)),
            dma((STEPS * CHUNKS + 3,)),
            dma,
            dma,
            dma,
            dma,
        ],
        compiler_params=pltpu.CompilerParams(collective_id=0, has_side_effects=True),
    )(
        stream,
        values_in,
        in_gate,
        out_gate,
        documents[None, :],
        conv_taps,
        head_gain[None, :],
        mix_weight,
        norm_gain[None, :],
        routes.T,
        route_weight.T,
        expert_gate,
        expert_up,
        expert_down.reshape(SIDE, SIDE, T, T),
        shared_gate,
        shared_up,
        shared_down,
    )


def solution(mesh):
    in_specs = (
        P("tp", "sp"),
        P("tp", "sp"),
        P("tp", "sp"),
        P("tp", "sp"),
        P("sp"),
        P(None, "tp"),
        P("tp"),
        P("tp", None),
        P("tp"),
        P("sp", None),
        P("sp", None),
        P("sp", None, "tp"),
        P("sp", None, "tp"),
        P("sp", None, "tp"),
        P(None, "tp"),
        P(None, "tp"),
        P("tp", None),
    )
    return jax.shard_map(
        local, mesh=mesh, in_specs=in_specs, out_specs=P("tp", "sp"), check_vma=False
    )
```

time: 94.2 us -> 81.9 us (0.87)
  Pallas kernels: 92.6 us -> 80.2 us
    pallas_call x1, Pallas kernels: 92.6 us -> 80.2 us  [local(): pl.pallas_call(kernel, name='layer', out_shape=jax.ShapeDtypeStruct((T, T...]
where the time goes in v3:
time: 81.9 us; the launch traced here: 81.6 us
  Pallas kernels  80.2 us (98%)
  local copies, waits for them, and re-layouts  1.38 us (2%)
    pallas_call x1, Pallas kernels, local(): pl.pallas_call(kernel, name='layer', out_shape=jax.ShapeDtypeStruct((T, T...  80.2 us

profile of v3, /device:TPU:1, one launch (start us, length us, event | category | flops | bytes accessed | tf_op | source)
XLA Modules:
  0.0 81.6 jit_solution(9140460304891011953)
XLA Ops:
  0.0 80.2 %layer.1 = bf16[128,128]{1,0:T(8,128)(2,1)} custom-call(bf16[128,128]{1,0:T(8,128)(2,1)} %stream.1, bf16[64,128]{1,0:T(8,128)(2,1)} %values_in.1, bf16[64,128]{1,0:T(8,128)(2,1)} %in_gate.1, bf16[64,128]{1,0:T(8,128)(2,1)} %out_gate.1, s32[1,128]{1,0:T(1,128)} %bitcast.9, f32[3,64]{1,0:T(4,128)} %conv_taps.1, f32[1,64]{1,0:T(1,128)} %bitcast.10, ...), custom_call_target="tpu_custom_call" | custom-call | tf_op jit(solution)/shard_map/layer/pallas_call | solution.py:583
  80.2 1.4 %copy.19 = bf16[128,128]{1,0:T(8,128)(2,1)} copy(bf16[128,128]{1,0:T(8,128)(2,1)} %layer.1) | data formatting | bytes 65536

commit v4 on v3

--- a/solution.py
+++ b/solution.py
@@ -25,9 +25,9 @@
 CHUNKS = len(DISTANCES)
 SIZES = [2 * len(chunk) for chunk in DISTANCES]
 STARTS = [sum(SIZES[:c]) for c in range(CHUNKS)]
-DIRECT = (True, False, True)
+DIRECT = (True, True, True)
 STEPS = 5
-LAG = 1.01
+LAG = 1.5
 SHARED = ((1, 0), (1, 1), (1, 3))
 SHARED_SEND_AFTER = (CHUNKS - 1, -2)
 
@@ -48,6 +48,24 @@
 
 
 def kernel(
+    stream_far,
+    values_in_far,
+    in_gate_far,
+    out_gate_far,
+    documents_far,
+    conv_taps_far,
+    head_gain_far,
+    mix_weight,
+    norm_gain_far,
+    routes_far,
+    route_weight_far,
+    expert_gate,
+    expert_up,
+    expert_down,
+    shared_gate,
+    shared_up,
+    shared_down,
+    out,
     stream,
     values_in,
     in_gate,
@@ -55,17 +73,9 @@
     documents,
     conv_taps,
     head_gain,
-    mix_weight,
     norm_gain,
     routes,
     route_weight,
-    expert_gate,
-    expert_up,
-    expert_down,
-    shared_gate,
-    shared_up,
-    shared_down,
-    out,
     halo_v,
     halo_g,
     halo_d,
@@ -93,6 +103,7 @@
     sh_part,
     sh_in,
     hidden,
+    told,
     load_sem,
     down_s,
     down_r,
@@ -134,10 +145,13 @@
 
     barrier = pltpu.get_barrier_semaphore()
 
-    @pl.loop(1, N_SP)
-    def _(step):
+    def along_z(dz, other):
+        return 2 * ((z + dz + N_Z) % N_Z) + (core + other) % 2
+
+    near = [(0, 1)] + [(dz, other) for dz in (-1, 1, -2, 2) for other in (0, 1)]
+    for dz, other in near:
         pl.semaphore_signal(
-            barrier, inc=1, device_id={"sp": (sp + step) % N_SP}, device_id_type=MESH
+            barrier, inc=1, device_id={"sp": along_z(dz, other)}, device_id_type=MESH
         )
 
     @pl.loop(1, N_TP)
@@ -150,6 +164,16 @@
         pltpu.make_async_copy(src, dst, load_sem.at[i])
         for i, (src, dst) in enumerate(
             [
+                (routes_far, routes),
+                (route_weight_far, route_weight),
+                (values_in_far, values_in),
+                (in_gate_far, in_gate),
+                (documents_far, documents),
+                (out_gate_far, out_gate),
+                (conv_taps_far, conv_taps),
+                (head_gain_far, head_gain),
+                (norm_gain_far, norm_gain),
+                (stream_far, stream),
                 (mix_weight, mix_here),
                 (expert_down, w_down),
                 (expert_down.at[y], w_one.at[y]),
@@ -164,7 +188,10 @@
     ]
     for load in loads:
         load.start()
-
+    small, loads = loads[:10], loads[10:]
+
+    for load in small[:2]:
+        load.wait()
     line = iota((T, T), 0)
     named = jnp.zeros((T, T), F32)
     weight = jnp.zeros((T, T), F32)
@@ -195,7 +222,18 @@
     comb_hi[...] = jnp.where(taken, dot(weight_hi, owner), 0.0).astype(BF16)
     comb_lo[...] = jnp.where(taken, dot(weight_lo, owner), 0.0).astype(BF16)
 
-    pl.semaphore_wait(barrier, N_SP + N_TP - 2)
+    pl.semaphore_wait(barrier, N_TP - 1 + len(near))
+
+    def tell(step):
+        for dz in (-2 << step, 2 << step):
+            pl.semaphore_signal(
+                told.at[step], inc=1, device_id={"sp": along_z(dz, 0)}, device_id_type=MESH
+            )
+
+    tell(0)
+
+    for load in small[2:]:
+        load.wait()
 
     behind = (sp + 1) % N_SP
     halos = [
@@ -267,6 +305,9 @@
     head_all[tp, first] = heads_after(product_before, docs_before)[:8]
     to_plane(lambda peer: head_all.at[tp, first], head_all.at[tp, first], tail_s, tail_r)
 
+    pl.semaphore_wait(told.at[0], 2)
+    tell(1)
+
     others = pl.ds(0, N_TP - 1)
     arrive(mix_w.at[others, pl.ds(0, HEAD // 2)], mix_r)
     swap = remote(mix_w.at[:, rows], mix_w.at[:, rows], swap_s, swap_r, sp=2 * z + 1 - core)
@@ -312,7 +353,8 @@
         )
 
     for dz, other in order:
-        disp_copy(dz, other).start()
+        if dz in DISTANCES[0]:
+            disp_copy(dz, other).start()
     own = core
     rows_all[y, x, own] = disp_out[sp]
 
@@ -495,6 +537,10 @@
             start_ret(chunk)
 
     go(normed_copies(0))
+    pl.semaphore_wait(told.at[1], 2)
+    for dz, other in order:
+        if dz not in DISTANCES[0]:
+            disp_copy(dz, other).start()
     to_plane(lambda peer: norm_gain, gains.at[tp], gain_s, gain_r)
     gains[tp] = norm_gain[...]
     steps = sorted(
@@ -584,9 +630,19 @@
         kernel,
         name="layer",
         out_shape=jax.ShapeDtypeStruct((T, T), BF16),
-        in_specs=[vmem] * 7 + [hbm] + [vmem] * 3 + [hbm] * 6,
+        in_specs=[hbm] * 17,
         out_specs=vmem,
         scratch_shapes=[
+            pltpu.VMEM((T, T), BF16),
+            pltpu.VMEM((HEAD, T), BF16),
+            pltpu.VMEM((HEAD, T), BF16),
+            pltpu.VMEM((HEAD, T), BF16),
+            pltpu.VMEM((1, T), jnp.int32),
+            pltpu.VMEM((3, HEAD), F32),
+            pltpu.VMEM((1, HEAD), F32),
+            pltpu.VMEM((1, T), F32),
+            pltpu.VMEM((TOP_K, T), jnp.int32),
+            pltpu.VMEM((TOP_K, T), F32),
             pltpu.VMEM((HEAD, T), BF16),
             pltpu.VMEM((HEAD, T), BF16),
             pltpu.VMEM((1, T), jnp.int32),
@@ -614,7 +670,8 @@
             pltpu.VMEM((N_TP, T, T), BF16),
             pltpu.VMEM((N_TP, T, T), BF16),
             pltpu.VMEM((T, T), F32),
-            dma((9,)),
+            pltpu.SemaphoreType.REGULAR((2,)),
+            dma((19,)),
             dma((2,)),
             dma((2,)),
             dma((3,)),

time: 81.9 us -> 78.8 us (0.962)
  Pallas kernels: 80.2 us -> 77.2 us
    pallas_call x1, Pallas kernels: 80.2 us -> 77.2 us  [local(): pl.pallas_call(kernel, name='layer', out_shape=jax.ShapeDtypeStruct((T, T...]
where the time goes in v4:
time: 78.8 us; the launch traced here: 78.6 us
  Pallas kernels  77.2 us (98%)
  local copies, waits for them, and re-layouts  1.38 us (2%)
    pallas_call x1, Pallas kernels, local(): pl.pallas_call(kernel, name='layer', out_shape=jax.ShapeDtypeStruct((T, T...  77.2 us

profile of v4, /device:TPU:1, one launch (start us, length us, event | category | flops | bytes accessed | tf_op | source)
XLA Modules:
  0.0 78.6 jit_solution(3676482425182447362)
XLA Ops:
  0.0 77.2 %layer.1 = bf16[128,128]{1,0:T(8,128)(2,1)} custom-call(bf16[128,128]{1,0:T(8,128)(2,1)} %stream_far.1, bf16[64,128]{1,0:T(8,128)(2,1)} %values_in_far.1, bf16[64,128]{1,0:T(8,128)(2,1)} %in_gate_far.1, bf16[64,128]{1,0:T(8,128)(2,1)} %out_gate_far.1, s32[1,128]{1,0:T(1,128)} %bitcast.9, f32[3,64]{1,0:T(4,128)} %conv_taps_far.1, f32[1,64]{1,0:T(1,128)} %bitcast.10, ...), custom_call_target="tpu_custom_call" | custom-call | tf_op jit(solution)/shard_map/layer/pallas_call | solution.py:629
  77.3 1.4 %copy.19 = bf16[128,128]{1,0:T(8,128)(2,1)} copy(bf16[128,128]{1,0:T(8,128)(2,1)} %layer.1) | data formatting | bytes 65536

commit v5 on v4

--- a/solution.py
+++ b/solution.py
@@ -27,8 +27,8 @@
 STARTS = [sum(SIZES[:c]) for c in range(CHUNKS)]
 DIRECT = (True, True, True)
 STEPS = 5
-LAG = 1.5
-SHARED = ((1, 0), (1, 1), (1, 3))
+LAG = 1.99
+SHARED = ((0, 1), (0, 2), (1, 2))
 SHARED_SEND_AFTER = (CHUNKS - 1, -2)
 
 

time: 78.8 us -> 80.4 us (1.020)
  Pallas kernels: 77.2 us -> 78.8 us
    pallas_call x1, Pallas kernels: 77.2 us -> 78.8 us  [local(): pl.pallas_call(kernel, name='layer', out_shape=jax.ShapeDtypeStruct((T, T...]
where the time goes in v5:
time: 80.4 us; the launch traced here: 80.2 us
  Pallas kernels  78.8 us (98%)
  local copies, waits for them, and re-layouts  1.38 us (2%)
    pallas_call x1, Pallas kernels, local(): pl.pallas_call(kernel, name='layer', out_shape=jax.ShapeDtypeStruct((T, T...  78.8 us

profile of v5, /device:TPU:1, one launch (start us, length us, event | category | flops | bytes accessed | tf_op | source)
XLA Modules:
  0.0 80.2 jit_solution(14054546007946437465)
XLA Ops:
  0.0 78.8 %layer.1 = bf16[128,128]{1,0:T(8,128)(2,1)} custom-call(bf16[128,128]{1,0:T(8,128)(2,1)} %stream_far.1, bf16[64,128]{1,0:T(8,128)(2,1)} %values_in_far.1, bf16[64,128]{1,0:T(8,128)(2,1)} %in_gate_far.1, bf16[64,128]{1,0:T(8,128)(2,1)} %out_gate_far.1, s32[1,128]{1,0:T(1,128)} %bitcast.9, f32[3,64]{1,0:T(4,128)} %conv_taps_far.1, f32[1,64]{1,0:T(1,128)} %bitcast.10, ...), custom_call_target="tpu_custom_call" | custom-call | tf_op jit(solution)/shard_map/layer/pallas_call | solution.py:629
  78.8 1.4 %copy.19 = bf16[128,128]{1,0:T(8,128)(2,1)} copy(bf16[128,128]{1,0:T(8,128)(2,1)} %layer.1) | data formatting | bytes 65536
